TPU v7x, 32 devices: a whole 2x2x4 slice. The times are simulated.
32 devices in a mesh: sp: 8 (over z, x), tp: 4 (over y, core).
Axes of the slice: x: 2, y: 2, z: 4, core: 2. Of those that a mesh axis runs over, the one named last changes fastest.
Arguments:
- residual: bfloat16 [2560, 2048], P(('sp', 'tp')), may hold values from -6 to 6
- query_narrow: bfloat16 [2560, 1024], P('sp', 'tp'), may hold values from -48 to 48
- key_narrow: bfloat16 [2560, 1024], P('sp', 'tp'), may hold values from -48 to 48
- value_narrow: bfloat16 [2560, 1024], P('sp', 'tp'), may hold values from -6 to 6
- query_wide: bfloat16 [2560, 2048], P('sp', 'tp'), may hold values from -48 to 48
- key_wide: bfloat16 [2560, 2048], P('sp', 'tp'), may hold values from -48 to 48
- value_wide: bfloat16 [2560, 1024], P('sp', 'tp'), may hold values from -6 to 6
- subtract_narrow: float32 [8], P('tp'), may hold values from 0.3 to 0.8
- subtract_wide: float32 [8], P('tp'), may hold values from 0.3 to 0.8
- head_gain: float32 [128], replicated, may hold values from 0.1 to 1.9
- out_narrow: bfloat16 [1024, 2048], replicated, may hold values from -0.125 to 0.125
- out_wide: bfloat16 [1024, 2048], replicated, may hold values from -0.125 to 0.125
- norm1_gain: float32 [2048], replicated, may hold values from 0.1 to 1.9
- norm2_gain: float32 [2048], replicated, may hold values from 0.1 to 1.9
- expert_ids: int32 [2560, 2], P(('sp', 'tp')), may hold values from 0 to 7, all different within a row; in each aligned block of 80 rows (0 to 79, 80 to 159, ...) at most 30 rows name the same one
- expert_weight: float32 [2560, 2], P(('sp', 'tp')), may hold values from 0.1 to 1
- gate_proj: bfloat16 [8, 2048, 2048], P('sp', None, 'tp'), may hold values from -0.125 to 0.125
- up_proj: bfloat16 [8, 2048, 2048], P('sp', None, 'tp'), may hold values from -0.125 to 0.125
- down_proj: bfloat16 [8, 2048, 2048], P('sp', 'tp'), may hold values from -0.125 to 0.125
Outputs:
- layer_out: bfloat16 [2560, 2048], P(('sp', 'tp'))
Inputs may be any that keep to these rules, and one draw needn't show every extreme that they name: `expert_ids`: each row names 2 different experts. Among the 80 rows of one device no expert is named more than 30 times, and in some device's rows some expert is named exactly 30 times.
All inputs are finite; a program needn't handle non-finite values.
Results may differ from a plain program's by a relative error of at most 0.014.
Values may be sent and summed in bfloat16 or wider, within the bound.
A program may use at most 128 MiB of HBM per device.

v0:
```python
import functools
import math

import jax
import jax.numpy as jnp
from jax import lax
from jax.experimental import pallas as pl
from jax.experimental.pallas import tpu as pltpu
from jax.sharding import PartitionSpec as P

residual_scale = 2.0**0.5


def layer_norm(values, gain):
    center = jnp.mean(values, -1, keepdims=True)
    spread = jnp.mean(jnp.square(values - center), -1, keepdims=True)
    return (values - center) * lax.rsqrt(spread + 1e-05) * gain


def block_take(shards, shard_rows):
    take = shards
    for count in range(shards, 0, -1):
        if shards % count == 0 and count * shard_rows >= 512:
            take = count
    return take


def start_carry(head_count, tok_rows, value_size):
    return (
        jnp.full((head_count, 2, tok_rows), -1e30, jnp.float32),
        jnp.zeros((head_count, 2, tok_rows), jnp.float32),
        jnp.zeros((head_count, 2, tok_rows, value_size), jnp.float32),
    )


def absorb_keys(carry, queries, key_piece, value_piece, shard_rows):
    head_count = queries.shape[1]
    key_size = queries.shape[3]
    shards = key_piece.shape[0] // shard_rows
    take = block_take(shards, shard_rows)
    span = take * shard_rows

    def one_block(step_index, state):
        rowtop, total, summed = state
        key_block = lax.dynamic_slice_in_dim(key_piece, step_index * span, span, 0).reshape(
            span, head_count, 2, key_size
        )
        value_block = lax.dynamic_slice_in_dim(value_piece, step_index * span, span, 0).reshape(
            span, head_count, -1
        )
        scores = jnp.einsum(
            "qhmd,khmd->hmqk", queries, key_block, preferred_element_type=jnp.float32
        ) * key_size ** (-0.5)
        newtop = jnp.maximum(rowtop, jnp.max(scores, -1))
        shrink = jnp.exp(rowtop - newtop)
        expo = jnp.exp(scores - newtop[..., None])
        total = total * shrink + jnp.sum(expo, -1)
        summed = summed * shrink[..., None] + jnp.einsum(
            "hmqk,khe->hmqe",
            expo.astype(jnp.bfloat16),
            value_block,
            preferred_element_type=jnp.float32,
        )
        return (newtop, total, summed)

    return lax.fori_loop(0, shards // take, one_block, carry)


def finish_heads(carry, subtract, head_gain):
    rowtop, total, summed = carry
    mapped = summed / total[..., None]
    diff = mapped[:, 0] - subtract[:, None, None] * mapped[:, 1]
    normed = diff * lax.rsqrt(jnp.mean(diff * diff, -1, keepdims=True) + 1e-06) * head_gain
    return jnp.transpose(normed, (1, 0, 2)).reshape(diff.shape[1], -1).astype(jnp.bfloat16)


def attend_kernel(
    head_count,
    scale_ref,
    query_ref,
    key_ref,
    value_ref,
    gain_ref,
    out_ref,
    query_all,
    key_all,
    value_all,
    key_turned,
    own,
    landed,
    send_sem,
    recv_sem,
    out_send,
    out_recv,
):
    shards, ranks = lax.axis_size("sp"), lax.axis_size("tp")
    me, rank = lax.axis_index("sp"), lax.axis_index("tp")
    tok_rows, value_size = key_ref.shape[0], gain_ref.shape[1]
    tasks = 2 * head_count
    splits = shards // tasks
    query_rows = tok_rows // splits
    out_rows = landed.shape[0]
    per_split = query_rows // out_rows
    pair = key_all.shape[1]
    size = pair // 2

    def pieces(target):
        task, split = target // splits, lax.rem(target, splits)
        return (
            query_ref.at[
                pl.ds(pl.multiple_of(split * query_rows, query_rows), query_rows),
                pl.ds(pl.multiple_of(task * pair, pair), pair),
            ],
            key_ref.at[:, pl.ds(pl.multiple_of(task * pair, pair), pair)],
            value_ref.at[:, pl.ds(pl.multiple_of(task * value_size, value_size), value_size)],
        )

    def places(source):
        return (
            query_all.at[pl.ds(pl.multiple_of(source * query_rows, query_rows), query_rows), :],
            key_all.at[pl.ds(pl.multiple_of(source * tok_rows, tok_rows), tok_rows), :],
            value_all.at[pl.ds(pl.multiple_of(source * tok_rows, tok_rows), tok_rows), :],
        )

    copies = []
    for hop in range(1, shards):
        target = lax.rem(me + hop, shards)
        for kind, (source, place) in enumerate(zip(pieces(target), places(me))):
            copies.append(
                pltpu.make_async_remote_copy(
                    src_ref=source,
                    dst_ref=place,
                    send_sem=send_sem.at[kind, hop],
                    recv_sem=recv_sem.at[kind, hop],
                    device_id={"sp": target},
                    device_id_type=pl.DeviceIdType.MESH,
                )
            )
            copies[-1].start()
    local = [
        pltpu.make_async_copy(source, place, recv_sem.at[kind, 0])
        for kind, (source, place) in enumerate(zip(pieces(me), places(me)))
    ]
    for copy in local:
        copy.start()
    for copy in local:
        copy.wait()
    for copy in copies:
        copy.wait()

    turn = math.gcd(key_all.shape[0], 256)

    @pl.loop(0, key_all.shape[0] // turn)
    def _(step):
        at = pl.ds(pl.multiple_of(step * turn, turn), turn)
        key_turned[:, at] = key_all[at, :].T

    my_task, my_split = me // splits, lax.rem(me, splits)
    my_group, my_head = my_task // head_count, lax.rem(my_task, head_count)
    column = my_group * (head_count * ranks) + rank * head_count + my_head
    factor, subtract = scale_ref[0, 0], scale_ref[0, 1]

    def to_tokens(block, part):
        source = own.at[
            pl.ds(pl.multiple_of(block * query_rows + part * out_rows, out_rows), out_rows), :
        ]
        place = landed.at[:, pl.ds(pl.multiple_of(column * value_size, value_size), value_size)]
        target = my_split * per_split + part
        remote = pltpu.make_async_remote_copy(
            src_ref=source,
            dst_ref=place,
            send_sem=out_send.at[block * per_split + part],
            recv_sem=out_recv.at[column],
            device_id={"sp": block, "tp": target},
            device_id_type=pl.DeviceIdType.MESH,
        )
        here = pltpu.make_async_copy(source, place, out_recv.at[column])
        return remote, here, (block == me) & (target == rank)

    @pl.loop(0, shards)
    def _(block):
        at = pl.ds(pl.multiple_of(block * query_rows, query_rows), query_rows)
        mapped = []
        for index in range(2):
            scores = jnp.dot(
                query_all[at, index * size : (index + 1) * size],
                key_turned[index * size : (index + 1) * size, :],
                preferred_element_type=jnp.float32,
            ) * factor
            expo = jnp.exp2(scores - jnp.max(scores, -1, keepdims=True))
            total = jnp.sum(expo, -1, keepdims=True)
            summed = jnp.dot(
                expo.astype(jnp.bfloat16), value_all[...], preferred_element_type=jnp.float32
            )
            mapped.append(summed / total)
        diff = mapped[0] - subtract * mapped[1]
        normed = diff * lax.rsqrt(jnp.mean(diff * diff, -1, keepdims=True) + 1e-06) * gain_ref[...]
        own[at, :] = normed.astype(jnp.bfloat16)
        for part in range(per_split):
            remote, here, mine = to_tokens(block, part)

            @pl.when(mine)
            def _():
                here.start()

            @pl.when(jnp.logical_not(mine))
            def _():
                remote.start()

    @pl.loop(0, shards)
    def _(block):
        for part in range(per_split):
            remote, here, mine = to_tokens(block, part)

            @pl.when(jnp.logical_not(mine))
            def _():
                remote.wait_send()

    for head in range(tasks * ranks):
        pltpu.make_async_copy(
            own.at[pl.ds(0, out_rows), :],
            landed.at[:, pl.ds(head * value_size, value_size)],
            out_recv.at[head],
        ).wait()
    out_ref[...] = landed[...]


def attend_by_head(
    queries, keys, values, subtract_narrow, subtract_wide, head_gain, out_rows
):
    shards, ranks = lax.axis_size("sp"), lax.axis_size("tp")
    me = lax.axis_index("sp")
    head_count, value_size = subtract_narrow.shape[0], head_gain.shape[0]
    tok_rows = keys[0].shape[0]
    narrow_size = keys[0].shape[1] // (2 * head_count)
    wide_size = keys[1].shape[1] // (2 * head_count)
    size = max(narrow_size, wide_size)
    splits = shards // (2 * head_count)

    def side_by_side(pair):
        padded = []
        for part in pair:
            maps = part.reshape(tok_rows, 2 * head_count, -1)
            maps = jnp.pad(maps, ((0, 0), (0, 0), (0, size - maps.shape[2])))
            padded.append(maps.reshape(tok_rows, -1))
        return jnp.concatenate(padded, 1)

    task = me // splits
    subtract = jnp.concatenate([subtract_narrow, subtract_wide])[task]
    scale = jnp.where(task < head_count, narrow_size ** (-0.5), wide_size ** (-0.5))
    scales = jnp.stack([scale * math.log2(math.e), subtract]).astype(jnp.float32)[None]
    tokens = shards * tok_rows
    query_total = tokens // splits
    heads = 2 * head_count * ranks
    vmem = pl.BlockSpec(memory_space=pltpu.VMEM)
    return pl.pallas_call(
        functools.partial(attend_kernel, head_count),
        out_shape=jax.ShapeDtypeStruct((out_rows, heads * value_size), jnp.bfloat16),
        in_specs=[pl.BlockSpec(memory_space=pltpu.SMEM)] + [vmem] * 4,
        out_specs=vmem,
        scratch_shapes=[
            pltpu.VMEM((query_total, 2 * size), jnp.bfloat16),
            pltpu.VMEM((tokens, 2 * size), jnp.bfloat16),
            pltpu.VMEM((tokens, value_size), jnp.bfloat16),
            pltpu.VMEM((2 * size, tokens), jnp.bfloat16),
            pltpu.VMEM((query_total, value_size), jnp.bfloat16),
            pltpu.VMEM((out_rows, heads * value_size), jnp.bfloat16),
            pltpu.SemaphoreType.DMA((3, shards)),
            pltpu.SemaphoreType.DMA((3, shards)),
            pltpu.SemaphoreType.DMA((query_total // out_rows,)),
            pltpu.SemaphoreType.DMA((heads,)),
        ],
        compiler_params=pltpu.CompilerParams(
            has_side_effects=True, vmem_limit_bytes=56 * 1024 * 1024
        ),
    )(
        scales,
        side_by_side(queries),
        side_by_side(keys),
        jnp.concatenate(values, 1),
        head_gain[None],
    )


def head_split_fits(tok_rows, out_rows, head_count, shards):
    tasks = 2 * head_count
    if shards % tasks or tok_rows % (shards // tasks) or tok_rows % 16 or out_rows % 16:
        return False
    query_rows = tok_rows // (shards // tasks)
    return query_rows % out_rows == 0


def expert_kernel(
    send_ref,
    gate_ref,
    up_ref,
    down_ref,
    out_ref,
    rows,
    part,
    pairs,
    mid,
    cross,
    done,
    back,
    far_send,
    far_recv,
    near_send,
    near_recv,
    sum_send,
    sum_recv,
    back_send,
    back_recv,
):
    shards, ranks = lax.axis_size("sp"), lax.axis_size("tp")
    me, rank = lax.axis_index("sp"), lax.axis_index("tp")
    cap = send_ref.shape[0] // shards
    side, core = rank // 2, lax.rem(rank, 2)
    partner, across = rank + 1 - 2 * core, lax.rem(rank + 2, ranks)
    my_place, far_place = core * 2 + side, core * 2 + 1 - side
    block = ranks * cap

    def at(ref, index, count=1):
        return ref.at[pl.ds(pl.multiple_of(index * cap, cap), count * cap), :]

    def copy_to(source, place, send, recv, device):
        return pltpu.make_async_remote_copy(
            src_ref=source,
            dst_ref=place,
            send_sem=send,
            recv_sem=recv,
            device_id=device,
            device_id_type=pl.DeviceIdType.MESH,
        )

    def far(hop):
        target = lax.rem(me + hop, shards)
        return copy_to(
            at(send_ref, target),
            at(rows, hop * ranks + my_place),
            far_send.at[hop],
            far_recv.at[hop],
            {"sp": target},
        )

    def near(kind, hop):
        place = far_place if kind == 2 else my_place
        piece = at(rows, hop * ranks + place)
        device = {"tp": across if kind == 1 else partner}
        return copy_to(piece, piece, near_send.at[kind, hop], near_recv.at[kind, hop], device)

    def pair_sum(hop):
        return copy_to(
            at(part, hop * ranks + (1 - core) * 2, 2),
            at(pairs, hop * 2, 2),
            sum_send.at[0, hop],
            sum_recv.at[0, hop],
            {"tp": partner},
        )

    def cross_sum(hop):
        return copy_to(
            at(mid, hop), at(cross, hop), sum_send.at[1, hop], sum_recv.at[1, hop], {"tp": across}
        )

    def give_back(hop):
        return copy_to(
            at(done, hop),
            at(back, me),
            back_send.at[hop],
            back_recv.at[hop],
            {"sp": lax.rem(me - hop + shards, shards)},
        )

    @pl.loop(1, shards)
    def _(hop):
        far(hop).start()

    own_rows = pltpu.make_async_copy(at(send_ref, me), at(rows, my_place), far_recv.at[0])
    own_rows.start()
    own_rows.wait()

    def share(hop):
        @pl.when(hop > 0)
        def _():
            far(hop).wait_recv()

        near(0, hop).start()
        near(1, hop).start()

    def relay(hop):
        near(1, hop).wait_recv()
        near(2, hop).start()

    def compute(hop):
        near(0, hop).wait_recv()
        near(2, hop).wait_recv()
        span = pl.ds(pl.multiple_of(hop * block, block), block)
        taken = rows[span, :]
        gate = jnp.dot(taken, gate_ref[...], preferred_element_type=jnp.float32)
        up = jnp.dot(taken, up_ref[...], preferred_element_type=jnp.float32)
        inner = (jax.nn.silu(gate) * up).astype(jnp.bfloat16)
        part[span, :] = jnp.dot(inner, down_ref[...], preferred_element_type=jnp.float32).astype(
            jnp.bfloat16
        )
        pair_sum(hop).start()

    def both(hop, place):
        mine = at(part, hop * ranks + core * 2 + place)[...].astype(jnp.float32)
        return mine + at(pairs, hop * 2 + place)[...].astype(jnp.float32)

    def add_pair(hop):
        pair_sum(hop).wait_recv()
        at(mid, hop)[...] = both(hop, 1 - side).astype(jnp.bfloat16)
        cross_sum(hop).start()

    def finish(hop):
        cross_sum(hop).wait_recv()
        total = both(hop, side) + at(cross, hop)[...].astype(jnp.float32)
        at(done, hop)[...] = total.astype(jnp.bfloat16)

        @pl.when(hop > 0)
        def _():
            give_back(hop).start()

    stages = (share, relay, compute, add_pair, finish)

    @pl.loop(0, shards + len(stages) - 1)
    def _(step):
        for late, stage in enumerate(stages):
            hop = step - late

            @pl.when((hop >= 0) & (hop < shards))
            def _():
                stage(hop)

    own_back = pltpu.make_async_copy(at(done, 0), at(back, me), back_recv.at[0])
    own_back.start()
    own_back.wait()

    @pl.loop(0, shards)
    def _(hop):
        for kind in range(3):
            near(kind, hop).wait_send()
        pair_sum(hop).wait_send()
        cross_sum(hop).wait_send()

        @pl.when(hop > 0)
        def _():
            far(hop).wait_send()
            give_back(hop).wait_send()
            copy_to(
                at(done, hop),
                at(back, lax.rem(me + hop, shards)),
                back_send.at[hop],
                back_recv.at[hop],
                {"sp": lax.rem(me + hop, shards)},
            ).wait_recv()

    out_ref[...] = back[...]


def experts_by_source(outgoing, gate, up, down):
    shards, ranks = lax.axis_size("sp"), lax.axis_size("tp")
    total, width = outgoing.shape
    vmem = pl.BlockSpec(memory_space=pltpu.VMEM)
    dma = pltpu.SemaphoreType.DMA
    return pl.pallas_call(
        expert_kernel,
        out_shape=jax.ShapeDtypeStruct((total, width), jnp.bfloat16),
        in_specs=[vmem] * 4,
        out_specs=vmem,
        scratch_shapes=[
            pltpu.VMEM((count * total, width), jnp.bfloat16)
            for count in (ranks, ranks, 2, 1, 1, 1, 1)
        ]
        + [
            dma((shards,)),
            dma((shards,)),
            dma((3, shards)),
            dma((3, shards)),
            dma((2, shards)),
            dma((2, shards)),
            dma((shards,)),
            dma((shards,)),
        ],
        compiler_params=pltpu.CompilerParams(
            has_side_effects=True, vmem_limit_bytes=56 * 1024 * 1024
        ),
    )(outgoing, gate, up, down)


def on_device(
    residual,
    query_narrow,
    key_narrow,
    value_narrow,
    query_wide,
    key_wide,
    value_wide,
    subtract_narrow,
    subtract_wide,
    head_gain,
    out_narrow,
    out_wide,
    norm1_gain,
    norm2_gain,
    expert_ids,
    expert_weight,
    gate_proj,
    up_proj,
    down_proj,
):
    tok_rows = query_narrow.shape[0]
    head_count = subtract_narrow.shape[0]
    value_size = head_gain.shape[0]
    if head_split_fits(tok_rows, residual.shape[0], head_count, lax.axis_size("sp")):
        attended = attend_by_head(
            (query_narrow, query_wide),
            (key_narrow, key_wide),
            (value_narrow, value_wide),
            subtract_narrow,
            subtract_wide,
            head_gain,
            residual.shape[0],
        )
        full_narrow, full_wide = jnp.split(attended, 2, 1)
    else:
        narrow_queries = query_narrow.reshape(tok_rows, head_count, 2, -1)
        wide_queries = query_wide.reshape(tok_rows, head_count, 2, -1)
        narrow_start = start_carry(head_count, tok_rows, value_size)
        wide_start = start_carry(head_count, tok_rows, value_size)
        narrow_state = absorb_keys(
            narrow_start,
            narrow_queries,
            lax.all_gather(key_narrow, "sp", axis=0, tiled=True),
            lax.all_gather(value_narrow, "sp", axis=0, tiled=True),
            tok_rows,
        )
        wide_state = absorb_keys(
            wide_start,
            wide_queries,
            lax.all_gather(key_wide, "sp", axis=0, tiled=True),
            lax.all_gather(value_wide, "sp", axis=0, tiled=True),
            tok_rows,
        )
        attended_narrow = finish_heads(narrow_state, subtract_narrow, head_gain)
        attended_wide = finish_heads(wide_state, subtract_wide, head_gain)
        full_narrow, full_wide = (
            lax.all_to_all(attended_narrow, "tp", split_axis=0, concat_axis=1, tiled=True),
            lax.all_to_all(attended_wide, "tp", split_axis=0, concat_axis=1, tiled=True),
        )
    mix = jnp.dot(full_narrow, out_narrow, preferred_element_type=jnp.float32) + jnp.dot(
        full_wide, out_wide, preferred_element_type=jnp.float32
    )
    hidden = layer_norm(residual_scale * residual.astype(jnp.float32) + mix, norm1_gain).astype(
        jnp.bfloat16
    )
    local_rows, top_count = expert_ids.shape
    experts = lax.axis_size("sp")
    capacity = max(2, 3 * local_rows * top_count // (2 * experts))
    in_kernel = lax.axis_size("tp") == 4 and 4 * experts * capacity * residual.shape[1] < 2**23
    if in_kernel:
        capacity = -(-capacity // 16) * 16
    flat_ids = expert_ids.reshape(-1)
    onehot = (flat_ids[:, None] == jnp.arange(experts, dtype=jnp.int32)[None, :]).astype(jnp.int32)
    before = jnp.cumsum(onehot, 0) - onehot
    position = jnp.sum(before * onehot, 1)
    slots = (flat_ids * capacity + position).reshape(local_rows, top_count)
    dispatch_table = jnp.any(
        jnp.arange(experts * capacity, dtype=jnp.int32)[:, None, None] == slots[None], -1
    ).astype(jnp.bfloat16)
    outgoing = jnp.dot(dispatch_table, hidden, preferred_element_type=jnp.float32).astype(
        jnp.bfloat16
    )
    if in_kernel:
        returned_flat = experts_by_source(outgoing, gate_proj[0], up_proj[0], down_proj[0])
        named = slots[..., None] == jnp.arange(experts * capacity, dtype=jnp.int32)
        combine = jnp.sum(jnp.where(named, expert_weight[..., None], 0.0), 1)
        routed = jnp.dot(
            combine, returned_flat.astype(jnp.float32), precision=lax.Precision.HIGHEST
        )
    else:
        outgoing = outgoing.reshape(experts, capacity, -1)
        gathered = lax.all_gather(
            lax.all_to_all(outgoing, "sp", split_axis=0, concat_axis=0, tiled=True),
            "tp",
            axis=1,
            tiled=True,
        )
        flat_rows = gathered.reshape(-1, gathered.shape[2])
        gate_part = jnp.dot(flat_rows, gate_proj[0], preferred_element_type=jnp.float32)
        up_part = jnp.dot(flat_rows, up_proj[0], preferred_element_type=jnp.float32)
        inner = (jax.nn.silu(gate_part) * up_part).astype(jnp.bfloat16)
        partial_out = jnp.dot(inner, down_proj[0], preferred_element_type=jnp.float32).reshape(
            gathered.shape
        )
        summed = lax.psum_scatter(
            partial_out.astype(jnp.bfloat16), "tp", scatter_dimension=1, tiled=True
        )
        returned = lax.all_to_all(summed, "sp", split_axis=0, concat_axis=0, tiled=True)
        returned_flat = returned.reshape(experts * capacity, -1)
        picked = returned_flat[slots].astype(jnp.float32)
        routed = jnp.sum(expert_weight[..., None] * picked, 1)
    return layer_norm(residual_scale * hidden.astype(jnp.float32) + routed, norm2_gain).astype(
        jnp.bfloat16
    )


def solution(mesh):
    placed = (
        P(("sp", "tp"), None),
        P("sp", "tp"),
        P("sp", "tp"),
        P("sp", "tp"),
        P("sp", "tp"),
        P("sp", "tp"),
        P("sp", "tp"),
        P("tp"),
        P("tp"),
        P(),
        P(),
        P(),
        P(),
        P(),
        P(("sp", "tp"), None),
        P(("sp", "tp"), None),
        P("sp", None, "tp"),
        P("sp", None, "tp"),
        P("sp", "tp", None),
    )
    return jax.shard_map(
        on_device, mesh=mesh, in_specs=placed, out_specs=P(("sp", "tp"), None), check_vma=False
    )
```

profile of v0, /device:TPU:0, one launch (start us, length us, event | category | flops | bytes accessed | tf_op | source)
XLA Modules:
  0.0 186.5 jit_solution(10074105403415684324)
XLA Ops:
  0.0 0.0 copy-start.4
  0.0 0.0 copy-start.5
  0.0 0.8 pad_maximum_fusion.3
  0.8 0.6 dynamic_slice.3
  1.4 1.2 maximum_bitcast_fusion.scale_ref
  2.6 1.1 copy.40
  3.7 0.2 copy.46
  3.9 0.0 copy-start.6
  3.9 0.0 copy-start.7
  3.9 1.1 copy.42
  5.1 0.2 copy.47
  5.3 0.0 copy-done.4
  5.3 0.0 copy-done.5
  5.3 0.0 copy-start
  5.3 1.3 pad_maximum_fusion
  6.6 0.0 copy-done.6
  6.6 0.0 copy-done.7
  6.6 0.7 pad_maximum_fusion.2.value_ref
  7.3 77.5 %shard_map.181 = bf16[80,2048]{1,0:T(8,128)(2,1)} custom-call(f32[1,2]{1,0:T(1,128)} %maximum_bitcast_fusion.scale_ref, bf16[320,1024]{1,0:T(8,128)(2,1)} %get-tuple-element.9.query_ref, bf16[320,1024]{1,0:T(8,128)(2,1)} %get-tuple-element.10.key_ref, bf16[320,512]{1,0:T(8,128)(2,1)} %pad_maximum_fusion.2.value_ref, f32[1,128]{1,0:T(1,128)} %bitcast.29), custom_call_target="tpu_custom_call" | custom-call | tf_op jit(solution)/shard_map/pallas_call | solution.py:256
  84.8 0.0 copy-done
  84.9 0.0 copy-start.1
  84.9 0.0 copy-start.2
  84.9 0.0 copy-start.3
  84.9 1.9 %fusion.2 = f32[80,2048]{1,0:T(8,128)S(1)} fusion(bf16[1024,2048]{1,0:T(8,128)(2,1)S(1)} %copy-done, bf16[80,2048]{1,0:T(8,128)(2,1)} %shard_map.181), kind=kOutput, calls=%fused_computation.15 | convolution fusion | flops 335544320 | bytes 5013504 | tf_op jit(solution)/shard_map/dot_general | solution.py:553
  86.8 0.3 copy-done.1
  87.1 0.0 copy-done.2
  87.2 0.1 copy-done.3
  87.3 1.0 fusion.7
  88.3 0.2 multiply_reduce_fusion.1
  88.5 0.0 copy-done.10
  88.6 0.1 copy.44
  88.7 0.1 eq.48
  88.8 0.6 reduce-window.6
  89.4 0.2 slice_reduce_fusion
  89.7 0.1 add_bitcast_fusion
  89.8 0.1 reduce_sum.59
  89.9 0.1 copy.45
  90.0 0.1 fusion.4
  90.1 0.0 copy-done.8
  90.1 1.5 convolution_convert_fusion.send_ref
  91.6 91.6 %shard_map.182 = bf16[256,2048]{1,0:T(8,128)(2,1)} custom-call(bf16[256,2048]{1,0:T(8,128)(2,1)} %convolution_convert_fusion.send_ref, bf16[2048,512]{1,0:T(8,128)(2,1)} %bitcast.22, bf16[2048,512]{1,0:T(8,128)(2,1)} %bitcast.23, bf16[512,2048]{1,0:T(8,128)(2,1)} %bitcast.24), custom_call_target="tpu_custom_call" | custom-call | tf_op jit(solution)/shard_map/pallas_call | solution.py:468
  183.2 0.0 copy-done.11
  183.2 0.0 copy-start.9
  183.2 0.1 select_reduce_fusion
  183.3 2.0 %fusion.8 = (f32[80]{0:T(128)S(1)}, f32[80,2048]{1,0:T(8,128)S(1)}) fusion(f32[80,256]{1,0:T(8,128)S(1)} %select_reduce_fusion, bf16[256,2048]{1,0:T(8,128)(2,1)} %shard_map.182, f32[2048]{0:T(1024)S(1)} %copy-done.8, f32[80]{0:T(128)S(1)} %add_rsqrt_fusion.1, f32[80,2048]{1,0:T(8,128)S(1)} %get-tuple-element.6, f32[80]{0:T(128)S(1)} %broadcast_multiply_fusion.1), kind=kOutput, calls=%fused_computation.34 | convolution fusion | flops 504627136 | bytes 2450368 | tf_op jit(solution)/shard_map/dot_general | solution.py:580
  185.4 0.2 multiply_reduce_fusion
  185.6 0.0 copy-done.9
  185.6 0.9 multiply_convert_fusion
  (15 shorter events, 0.2 us)
Async XLA Ops:
  0.0 5.3 %copy-start.4 = (bf16[320,512]{1,0:T(8,128)(2,1)S(1)}, bf16[320,512]{1,0:T(8,128)(2,1)}, u32[]{:S(2)}) copy-start(bf16[320,512]{1,0:T(8,128)(2,1)} %param.23) | copy-start | bytes 983044
  0.0 5.3 %copy-start.5 = (bf16[320,512]{1,0:T(8,128)(2,1)S(1)}, bf16[320,512]{1,0:T(8,128)(2,1)}, u32[]{:S(2)}) copy-start(bf16[320,512]{1,0:T(8,128)(2,1)} %param.24) | copy-start | bytes 983044
  3.9 2.7 %copy-start.6 = (bf16[320,256]{1,0:T(8,128)(2,1)S(1)}, bf16[320,256]{1,0:T(8,128)(2,1)}, u32[]{:S(2)}) copy-start(bf16[320,256]{1,0:T(8,128)(2,1)} %param.25) | copy-start | bytes 491524
  3.9 2.7 %copy-start.7 = (bf16[320,256]{1,0:T(8,128)(2,1)S(1)}, bf16[320,256]{1,0:T(8,128)(2,1)}, u32[]{:S(2)}) copy-start(bf16[320,256]{1,0:T(8,128)(2,1)} %param.22) | copy-start | bytes 491524
  5.3 79.6 %copy-start = (bf16[1024,2048]{1,0:T(8,128)(2,1)S(1)}, bf16[1024,2048]{1,0:T(8,128)(2,1)}, u32[]{:S(2)}) copy-start(bf16[1024,2048]{1,0:T(8,128)(2,1)} %param.29) | copy-start | bytes 12582916
  84.9 2.3 %copy-start.1 = (bf16[1024,2048]{1,0:T(8,128)(2,1)S(1)}, bf16[1024,2048]{1,0:T(8,128)(2,1)}, u32[]{:S(2)}) copy-start(bf16[1024,2048]{1,0:T(8,128)(2,1)} %param.30) | copy-start | bytes 12582916
  84.9 2.3 %copy-start.2 = (bf16[80,2048]{1,0:T(8,128)(2,1)S(1)}, bf16[80,2048]{1,0:T(8,128)(2,1)}, u32[]{:S(2)}) copy-start(bf16[80,2048]{1,0:T(8,128)(2,1)} %shard_map.181) | copy-start | bytes 983044
  84.9 2.4 %copy-start.3 = (bf16[80,2048]{1,0:T(8,128)(2,1)S(1)}, bf16[80,2048]{1,0:T(8,128)(2,1)}, u32[]{:S(2)}) copy-start(bf16[80,2048]{1,0:T(8,128)(2,1)} %param.19) | copy-start | bytes 983044
  87.3 1.3 copy-start.10
  87.3 2.8 %copy-start.8 = (f32[2048]{0:T(1024)S(1)}, f32[2048]{0:T(1024)}, u32[]{:S(2)}) copy-start(f32[2048]{0:T(1024)} %param.31) | copy-start | bytes 24580
  91.6 91.6 %copy-start.11 = (f32[80,2]{0,1:T(2,128)S(1)}, f32[80,2]{0,1:T(2,128)}, u32[]{:S(2)}) copy-start(f32[80,2]{0,1:T(2,128)} %param.34) | copy-start | bytes 1924
  183.2 2.4 %copy-start.9 = (f32[2048]{0:T(1024)S(1)}, f32[2048]{0:T(1024)}, u32[]{:S(2)}) copy-start(f32[2048]{0:T(1024)} %param.32) | copy-start | bytes 24580
where the time goes:
time: 187 us
  Pallas kernels  169 us (90%)
  matrix products  6.46 us (3%)
  other arithmetic  6.37 us (3%)
  local copies, waits for them, and re-layouts  4.38 us (2%)
    pallas_call x1, Pallas kernels, experts_by_source(): pl.pallas_call(expert_kernel, out_shape=jax.ShapeDtypeStruct((total, widt...  91.6 us
    pallas_call x1, Pallas kernels, attend_by_head(): pl.pallas_call(functools.partial(attend_kernel, head_count), out_shape=ja...  77.5 us

commit v1 on v0

--- a/solution.py
+++ b/solution.py
@@ -75,129 +75,182 @@
 
 
 def attend_kernel(
-    head_count,
-    scale_ref,
-    query_ref,
-    key_ref,
-    value_ref,
+    narrow_sub_ref,
+    wide_sub_ref,
     gain_ref,
+    query_narrow_ref,
+    key_narrow_ref,
+    value_narrow_ref,
+    query_wide_ref,
+    key_wide_ref,
+    value_wide_ref,
     out_ref,
     query_all,
     key_all,
     value_all,
-    key_turned,
     own,
     landed,
     send_sem,
     recv_sem,
+    pass_send,
+    pass_recv,
     out_send,
     out_recv,
 ):
-    shards, ranks = lax.axis_size("sp"), lax.axis_size("tp")
+    ranks = lax.axis_size("tp")
     me, rank = lax.axis_index("sp"), lax.axis_index("tp")
-    tok_rows, value_size = key_ref.shape[0], gain_ref.shape[1]
-    tasks = 2 * head_count
-    splits = shards // tasks
-    query_rows = tok_rows // splits
-    out_rows = landed.shape[0]
-    per_split = query_rows // out_rows
-    pair = key_all.shape[1]
-    size = pair // 2
-
-    def pieces(target):
-        task, split = target // splits, lax.rem(target, splits)
+    layer, side = me // 2, lax.rem(me, 2)
+    partner = me + 1 - 2 * side
+    tok_rows = key_narrow_ref.shape[0]
+    head_count = narrow_sub_ref.shape[0]
+    layers = 2 * head_count
+    out_rows, lanes = landed.shape[0], gain_ref.shape[1]
+    narrow_size = lanes // 2
+
+    def is_wide(index):
+        return lax.rem((index + 1) // 2, 2) if not isinstance(index, int) else (index + 1) // 2 % 2
+
+    wide, my_head = is_wide(layer), layer // 2
+
+    def visit(step):
         return (
-            query_ref.at[
-                pl.ds(pl.multiple_of(split * query_rows, query_rows), query_rows),
-                pl.ds(pl.multiple_of(task * pair, pair), pair),
-            ],
-            key_ref.at[:, pl.ds(pl.multiple_of(task * pair, pair), pair)],
-            value_ref.at[:, pl.ds(pl.multiple_of(task * value_size, value_size), value_size)],
-        )
-
-    def places(source):
-        return (
-            query_all.at[pl.ds(pl.multiple_of(source * query_rows, query_rows), query_rows), :],
-            key_all.at[pl.ds(pl.multiple_of(source * tok_rows, tok_rows), tok_rows), :],
-            value_all.at[pl.ds(pl.multiple_of(source * tok_rows, tok_rows), tok_rows), :],
-        )
-
-    copies = []
-    for hop in range(1, shards):
-        target = lax.rem(me + hop, shards)
-        for kind, (source, place) in enumerate(zip(pieces(target), places(me))):
-            copies.append(
-                pltpu.make_async_remote_copy(
-                    src_ref=source,
-                    dst_ref=place,
-                    send_sem=send_sem.at[kind, hop],
-                    recv_sem=recv_sem.at[kind, hop],
-                    device_id={"sp": target},
-                    device_id_type=pl.DeviceIdType.MESH,
-                )
-            )
-            copies[-1].start()
-    local = [
-        pltpu.make_async_copy(source, place, recv_sem.at[kind, 0])
-        for kind, (source, place) in enumerate(zip(pieces(me), places(me)))
-    ]
-    for copy in local:
-        copy.start()
-    for copy in local:
-        copy.wait()
-    for copy in copies:
-        copy.wait()
-
-    turn = math.gcd(key_all.shape[0], 256)
-
-    @pl.loop(0, key_all.shape[0] // turn)
-    def _(step):
-        at = pl.ds(pl.multiple_of(step * turn, turn), turn)
-        key_turned[:, at] = key_all[at, :].T
-
-    my_task, my_split = me // splits, lax.rem(me, splits)
-    my_group, my_head = my_task // head_count, lax.rem(my_task, head_count)
-    column = my_group * (head_count * ranks) + rank * head_count + my_head
-    factor, subtract = scale_ref[0, 0], scale_ref[0, 1]
-
-    def to_tokens(block, part):
-        source = own.at[
-            pl.ds(pl.multiple_of(block * query_rows + part * out_rows, out_rows), out_rows), :
-        ]
-        place = landed.at[:, pl.ds(pl.multiple_of(column * value_size, value_size), value_size)]
-        target = my_split * per_split + part
+            layer,
+            layer + 1 - 2 * lax.rem(layer, 2),
+            lax.rem(layer + 2, layers),
+            layers - 1 - layer,
+        )[step]
+
+    def piece(kind, target):
+        head = target // 2
+        value = pl.ds(head * lanes, lanes)
+        if not is_wide(target):
+            return (key_narrow_ref, None, value_narrow_ref, query_narrow_ref, None)[kind].at[:, value]
+        if kind == 2:
+            return value_wide_ref.at[:, value]
+        ref = key_wide_ref if kind < 2 else query_wide_ref
+        return ref.at[:, pl.ds((2 * head + kind % 3) * lanes, lanes)]
+
+    def place(kind, index, half):
+        row = 2 * index + half if kind < 3 else index
+        at = pl.ds(pl.multiple_of(row * tok_rows, tok_rows), tok_rows)
+        if kind == 2:
+            return value_all.at[at, pl.ds(0, lanes)]
+        return key_all.at[kind, at, :] if kind < 2 else query_all.at[kind - 3, at, :]
+
+    def when_mine(kind, action):
+        if kind in (1, 4):
+            pl.when(wide == 1)(action)
+        else:
+            action()
+
+    def to_layer(kind, target):
+        return pltpu.make_async_remote_copy(
+            src_ref=piece(kind, target),
+            dst_ref=place(kind, layer, side),
+            send_sem=send_sem.at[kind, target],
+            recv_sem=recv_sem.at[kind, layer],
+            device_id={"sp": 2 * target + side},
+            device_id_type=pl.DeviceIdType.MESH,
+        )
+
+    def kinds_for(target, kinds):
+        return [kind for kind in kinds if is_wide(target) or kind not in (1, 4)]
+
+    for kinds in ((0, 1, 2), (3, 4)):
+        for target in sorted(range(layers), key=lambda index: -is_wide(index)):
+            for kind in kinds_for(target, kinds):
+
+                @pl.when(layer != target)
+                def _():
+                    to_layer(kind, target).start()
+
+                @pl.when(layer == target)
+                def _():
+                    pltpu.make_async_copy(
+                        piece(kind, target), place(kind, target, side), recv_sem.at[kind, target]
+                    ).start()
+
+    value_all[:, lanes:] = jnp.ones((value_all.shape[0], lanes), jnp.bfloat16)
+
+    def landed_here(kind, index, half, sem):
+        where = place(kind, index, half)
+        pltpu.make_async_copy(where, where, sem.at[kind, index]).wait()
+
+    def pass_on(kind, index):
+        where = place(kind, index, side)
+        return pltpu.make_async_remote_copy(
+            src_ref=where,
+            dst_ref=where,
+            send_sem=pass_send.at[kind, index],
+            recv_sem=pass_recv.at[kind, index],
+            device_id={"sp": partner},
+            device_id_type=pl.DeviceIdType.MESH,
+        )
+
+    for step in range(layers):
+        index = visit(step)
+        for kind in range(3):
+
+            def forward():
+                landed_here(kind, index, side, recv_sem)
+                pass_on(kind, index).start()
+
+            when_mine(kind, forward)
+    for step in range(layers):
+        index = visit(step)
+        for kind in range(3):
+            when_mine(kind, lambda: landed_here(kind, index, 1 - side, pass_recv))
+
+    scale = math.log2(math.e) * jnp.where(wide == 1, lanes ** (-0.5), narrow_size ** (-0.5))
+    scale = scale.astype(jnp.float32)
+    subtract = jnp.where(wide == 1, wide_sub_ref[my_head], narrow_sub_ref[my_head])
+    column = wide * (head_count * ranks) + rank * head_count + my_head
+
+    def to_tokens(index, part):
+        row = pl.multiple_of(index * tok_rows + part * out_rows, out_rows)
+        source = own.at[pl.ds(row, out_rows), :]
+        there = landed.at[:, pl.ds(pl.multiple_of(column * lanes, lanes), lanes)]
+        block = 2 * index + side
         remote = pltpu.make_async_remote_copy(
             src_ref=source,
-            dst_ref=place,
-            send_sem=out_send.at[block * per_split + part],
+            dst_ref=there,
+            send_sem=out_send.at[index, part],
             recv_sem=out_recv.at[column],
-            device_id={"sp": block, "tp": target},
+            device_id={"sp": block, "tp": part},
             device_id_type=pl.DeviceIdType.MESH,
         )
-        here = pltpu.make_async_copy(source, place, out_recv.at[column])
-        return remote, here, (block == me) & (target == rank)
-
-    @pl.loop(0, shards)
-    def _(block):
-        at = pl.ds(pl.multiple_of(block * query_rows, query_rows), query_rows)
+        here = pltpu.make_async_copy(source, there, out_recv.at[column])
+        return remote, here, (block == me) & (rank == part)
+
+    lane = lax.broadcasted_iota(jnp.int32, (tok_rows, lanes), 1)
+    for step in range(layers):
+        index = visit(step)
+        for kind in (3, 4):
+            when_mine(kind, lambda: landed_here(kind, index, side, recv_sem))
+        at = pl.ds(pl.multiple_of(index * tok_rows, tok_rows), tok_rows)
         mapped = []
-        for index in range(2):
-            scores = jnp.dot(
-                query_all[at, index * size : (index + 1) * size],
-                key_turned[index * size : (index + 1) * size, :],
+        for part in range(2):
+            low = jnp.where(wide == 1, 0, part * narrow_size)
+            high = jnp.where(wide == 1, lanes, (part + 1) * narrow_size)
+            plane = part * wide
+            queries = jnp.where(
+                (lane >= low) & (lane < high), query_all[plane, at, :].astype(jnp.float32), 0.0
+            ).astype(jnp.bfloat16)
+            scores = lax.dot_general(
+                queries,
+                key_all[plane],
+                (((1,), (1,)), ((), ())),
                 preferred_element_type=jnp.float32,
-            ) * factor
-            expo = jnp.exp2(scores - jnp.max(scores, -1, keepdims=True))
-            total = jnp.sum(expo, -1, keepdims=True)
-            summed = jnp.dot(
-                expo.astype(jnp.bfloat16), value_all[...], preferred_element_type=jnp.float32
             )
-            mapped.append(summed / total)
+            top = jnp.max(scores, -1, keepdims=True)
+            expo = jnp.exp2(scores * scale - top * scale).astype(jnp.bfloat16)
+            summed = jnp.dot(expo, value_all[...], preferred_element_type=jnp.float32)
+            mapped.append(summed[:, :lanes] / summed[:, lanes:])
         diff = mapped[0] - subtract * mapped[1]
         normed = diff * lax.rsqrt(jnp.mean(diff * diff, -1, keepdims=True) + 1e-06) * gain_ref[...]
         own[at, :] = normed.astype(jnp.bfloat16)
-        for part in range(per_split):
-            remote, here, mine = to_tokens(block, part)
+        for part in range(ranks):
+            remote, here, mine = to_tokens(index, part)
 
             @pl.when(mine)
             def _():
@@ -207,87 +260,82 @@
             def _():
                 remote.start()
 
-    @pl.loop(0, shards)
-    def _(block):
-        for part in range(per_split):
-            remote, here, mine = to_tokens(block, part)
+    for target in range(layers):
+        for kind in kinds_for(target, range(5)):
+
+            @pl.when(layer != target)
+            def _():
+                to_layer(kind, target).wait_send()
+
+    for index in range(layers):
+        for kind in range(3):
+            when_mine(kind, lambda: pass_on(kind, index).wait_send())
+        for part in range(ranks):
+            remote, here, mine = to_tokens(index, part)
 
             @pl.when(jnp.logical_not(mine))
             def _():
                 remote.wait_send()
 
-    for head in range(tasks * ranks):
-        pltpu.make_async_copy(
-            own.at[pl.ds(0, out_rows), :],
-            landed.at[:, pl.ds(head * value_size, value_size)],
-            out_recv.at[head],
-        ).wait()
+    for head in range(layers * ranks):
+        where = landed.at[:, pl.ds(head * lanes, lanes)]
+        pltpu.make_async_copy(where, where, out_recv.at[head]).wait()
     out_ref[...] = landed[...]
 
 
-def attend_by_head(
-    queries, keys, values, subtract_narrow, subtract_wide, head_gain, out_rows
-):
+def attend_by_head(queries, keys, values, subtract_narrow, subtract_wide, head_gain, out_rows):
     shards, ranks = lax.axis_size("sp"), lax.axis_size("tp")
-    me = lax.axis_index("sp")
-    head_count, value_size = subtract_narrow.shape[0], head_gain.shape[0]
+    head_count, lanes = subtract_narrow.shape[0], head_gain.shape[0]
     tok_rows = keys[0].shape[0]
-    narrow_size = keys[0].shape[1] // (2 * head_count)
-    wide_size = keys[1].shape[1] // (2 * head_count)
-    size = max(narrow_size, wide_size)
-    splits = shards // (2 * head_count)
-
-    def side_by_side(pair):
-        padded = []
-        for part in pair:
-            maps = part.reshape(tok_rows, 2 * head_count, -1)
-            maps = jnp.pad(maps, ((0, 0), (0, 0), (0, size - maps.shape[2])))
-            padded.append(maps.reshape(tok_rows, -1))
-        return jnp.concatenate(padded, 1)
-
-    task = me // splits
-    subtract = jnp.concatenate([subtract_narrow, subtract_wide])[task]
-    scale = jnp.where(task < head_count, narrow_size ** (-0.5), wide_size ** (-0.5))
-    scales = jnp.stack([scale * math.log2(math.e), subtract]).astype(jnp.float32)[None]
-    tokens = shards * tok_rows
-    query_total = tokens // splits
-    heads = 2 * head_count * ranks
+    tokens, layers = shards * tok_rows, 2 * head_count
+    heads = layers * ranks
     vmem = pl.BlockSpec(memory_space=pltpu.VMEM)
+    smem = pl.BlockSpec(memory_space=pltpu.SMEM)
+    dma = pltpu.SemaphoreType.DMA
     return pl.pallas_call(
-        functools.partial(attend_kernel, head_count),
-        out_shape=jax.ShapeDtypeStruct((out_rows, heads * value_size), jnp.bfloat16),
-        in_specs=[pl.BlockSpec(memory_space=pltpu.SMEM)] + [vmem] * 4,
+        attend_kernel,
+        out_shape=jax.ShapeDtypeStruct((out_rows, heads * lanes), jnp.bfloat16),
+        in_specs=[smem, smem, vmem] + [pl.BlockSpec(memory_space=pl.ANY)] * 6,
         out_specs=vmem,
         scratch_shapes=[
-            pltpu.VMEM((query_total, 2 * size), jnp.bfloat16),
-            pltpu.VMEM((tokens, 2 * size), jnp.bfloat16),
-            pltpu.VMEM((tokens, value_size), jnp.bfloat16),
-            pltpu.VMEM((2 * size, tokens), jnp.bfloat16),
-            pltpu.VMEM((query_total, value_size), jnp.bfloat16),
-            pltpu.VMEM((out_rows, heads * value_size), jnp.bfloat16),
-            pltpu.SemaphoreType.DMA((3, shards)),
-            pltpu.SemaphoreType.DMA((3, shards)),
-            pltpu.SemaphoreType.DMA((query_total // out_rows,)),
-            pltpu.SemaphoreType.DMA((heads,)),
+            pltpu.VMEM((2, layers * tok_rows, lanes), jnp.bfloat16),
+            pltpu.VMEM((2, tokens, lanes), jnp.bfloat16),
+            pltpu.VMEM((tokens, 2 * lanes), jnp.bfloat16),
+            pltpu.VMEM((layers * tok_rows, lanes), jnp.bfloat16),
+            pltpu.VMEM((out_rows, heads * lanes), jnp.bfloat16),
+            dma((5, layers)),
+            dma((5, layers)),
+            dma((3, layers)),
+            dma((3, layers)),
+            dma((layers, ranks)),
+            dma((heads,)),
         ],
         compiler_params=pltpu.CompilerParams(
-            has_side_effects=True, vmem_limit_bytes=56 * 1024 * 1024
+            has_side_effects=True, vmem_limit_bytes=40 * 1024 * 1024
         ),
     )(
-        scales,
-        side_by_side(queries),
-        side_by_side(keys),
-        jnp.concatenate(values, 1),
+        subtract_narrow,
+        subtract_wide,
         head_gain[None],
-    )
-
-
-def head_split_fits(tok_rows, out_rows, head_count, shards):
-    tasks = 2 * head_count
-    if shards % tasks or tok_rows % (shards // tasks) or tok_rows % 16 or out_rows % 16:
-        return False
-    query_rows = tok_rows // (shards // tasks)
-    return query_rows % out_rows == 0
+        queries[0],
+        keys[0],
+        values[0],
+        queries[1],
+        keys[1],
+        values[1],
+    )
+
+
+def head_split_fits(tok_rows, out_rows, ranks, heads, shards, value_size, key_sizes):
+    return (
+        heads == 2
+        and shards == 4 * heads
+        and out_rows * ranks == tok_rows
+        and tok_rows % 16 == 0
+        and out_rows % 16 == 0
+        and value_size == 128
+        and key_sizes == (value_size // 2, value_size)
+    )
 
 
 def expert_kernel(
@@ -514,7 +562,15 @@
     tok_rows = query_narrow.shape[0]
     head_count = subtract_narrow.shape[0]
     value_size = head_gain.shape[0]
-    if head_split_fits(tok_rows, residual.shape[0], head_count, lax.axis_size("sp")):
+    if head_split_fits(
+        tok_rows,
+        residual.shape[0],
+        lax.axis_size("tp"),
+        head_count,
+        lax.axis_size("sp"),
+        value_size,
+        tuple(part.shape[1] // (2 * head_count) for part in (key_narrow, key_wide)),
+    ):
         attended = attend_by_head(
             (query_narrow, query_wide),
             (key_narrow, key_wide),

time: 187 us -> 154 us (0.82)
  Pallas kernels: 169 us -> 136 us
  other arithmetic: 6.37 us -> 2.35 us
  local copies, waits for them, and re-layouts: 4.38 us -> 8.26 us
    pallas_call x1, Pallas kernels: 77.5 us -> 57.6 us  [attend_by_head(): pl.pallas_call(attend_kernel, out_shape=jax.ShapeDtypeStruct((out_rows, h...]
    pallas_call x1, Pallas kernels: 91.6 us -> 78 us  [experts_by_source(): pl.pallas_call(expert_kernel, out_shape=jax.ShapeDtypeStruct((total, widt...]
    unnamed x27 -> x31, local copies, waits for them, and re-layouts: 2.82 us -> 7.7 us
    concatenate x3 -> x0, other arithmetic: 2.82 us -> none  [the longest x1 1.26 us: side_by_side(): return jnp.concatenate(padded, 1)]
where the time goes in v1:
time: 154 us
  Pallas kernels  136 us (88%)
  local copies, waits for them, and re-layouts  8.26 us (5%)
  matrix products  7.58 us (5%)
  other arithmetic  2.35 us (2%)
    pallas_call x1, Pallas kernels, experts_by_source(): pl.pallas_call(expert_kernel, out_shape=jax.ShapeDtypeStruct((total, widt...  78 us
    pallas_call x1, Pallas kernels, attend_by_head(): pl.pallas_call(attend_kernel, out_shape=jax.ShapeDtypeStruct((out_rows, h...  57.6 us
    unnamed x31, local copies, waits for them, and re-layouts  7.7 us

profile of v1, /device:TPU:0, one launch (start us, length us, event | category | flops | bytes accessed | tf_op | source)
XLA Modules:
  0.0 154.0 jit_solution(18118665658092587217)
XLA Ops:
  0.0 0.0 copy-start
  0.0 1.0 copy-done
  1.0 0.0 copy-start.1
  1.0 1.0 copy-done.1
  1.9 0.0 copy-start.2
  1.9 0.9 copy-done.2
  2.9 0.0 copy-start.3
  2.9 0.9 copy-done.3
  3.8 0.0 copy-start.4
  3.8 0.9 copy-done.4
  4.7 0.0 copy-start.5
  4.7 0.9 copy-done.5
  5.6 0.0 copy-start.6
  5.6 0.7 copy-done.6
  6.3 0.0 copy-start.7
  6.3 0.7 copy-done.7
  6.9 0.0 copy-start.8
  6.9 0.7 copy-done.8
  7.6 0.0 copy-start.9
  7.6 0.0 copy-start.10
  7.6 57.6 %shard_map.181 = bf16[80,2048]{1,0:T(8,128)(2,1)S(1)} custom-call(f32[2]{0:T(128)S(1)} %copy-done.6, f32[2]{0:T(128)S(1)} %copy-done.7, f32[1,128]{1,0:T(1,128)S(1)} %bitcast.15, bf16[320,256]{1,0:T(8,128)(2,1)S(1)} %copy-done.2, bf16[320,256]{1,0:T(8,128)(2,1)S(1)} %copy-done.3, bf16[320,256]{1,0:T(8,128)(2,1)S(1)} %copy-done.4, ...), custom_call_target="tpu_custom_call" | custom-call | tf_op jit(solution)/shard_map/pallas_call | solution.py:295
  65.2 3.0 %fusion.2 = f32[80,2048]{1,0:T(8,128)S(1)} fusion(bf16[1024,2048]{1,0:T(8,128)(2,1)} %param.29, bf16[80,2048]{1,0:T(8,128)(2,1)S(1)} %shard_map.181), kind=kOutput, calls=%fused_computation.12 | convolution fusion | flops 335544320 | bytes 5013504 | tf_op jit(solution)/shard_map/dot_general | solution.py:609
  68.2 0.0 copy-done.9
  68.2 0.0 copy-done.10
  68.3 0.0 copy-start.13
  68.3 0.0 copy-start.11
  68.3 1.0 fusion.7
  69.3 0.2 multiply_reduce_fusion.1
  69.5 0.0 copy-done.13
  69.5 0.1 copy.32
  69.6 0.1 eq.48
  69.8 0.6 reduce-window.6
  70.4 0.2 slice_reduce_fusion
  70.7 0.1 add_bitcast_fusion
  70.8 0.1 reduce_sum.59
  70.9 0.1 copy.33
  71.0 0.1 fusion.4
  71.1 0.0 copy-done.11
  71.1 1.5 convolution_convert_fusion.send_ref
  72.6 0.0 copy-start.14
  72.6 0.0 copy-start.12
  72.6 78.0 %shard_map.182 = bf16[256,2048]{1,0:T(8,128)(2,1)} custom-call(bf16[256,2048]{1,0:T(8,128)(2,1)} %convolution_convert_fusion.send_ref, bf16[2048,512]{1,0:T(8,128)(2,1)} %bitcast.16, bf16[2048,512]{1,0:T(8,128)(2,1)} %bitcast.17, bf16[512,2048]{1,0:T(8,128)(2,1)} %bitcast.18), custom_call_target="tpu_custom_call" | custom-call | tf_op jit(solution)/shard_map/pallas_call | solution.py:516
  150.7 0.0 copy-done.14
  150.7 0.1 select_reduce_fusion
  150.8 2.0 %fusion.8 = (f32[80]{0:T(128)S(1)}, f32[80,2048]{1,0:T(8,128)S(1)}) fusion(f32[80,256]{1,0:T(8,128)S(1)} %select_reduce_fusion, bf16[256,2048]{1,0:T(8,128)(2,1)} %shard_map.182, f32[2048]{0:T(1024)S(1)} %copy-done.11, f32[80]{0:T(128)S(1)} %add_rsqrt_fusion.1, f32[80,2048]{1,0:T(8,128)S(1)} %get-tuple-element.6, f32[80]{0:T(128)S(1)} %broadcast_multiply_fusion.1), kind=kOutput, calls=%fused_computation.29 | convolution fusion | flops 504627136 | bytes 2450368 | tf_op jit(solution)/shard_map/dot_general | solution.py:636
  152.8 0.2 multiply_reduce_fusion
  153.1 0.0 copy-done.12
  153.1 0.9 multiply_convert_fusion
  (10 shorter events, 0.1 us)
Async XLA Ops:
  0.0 1.0 copy-start
  1.0 1.0 copy-start.1
  1.9 0.9 copy-start.2
  2.9 0.9 copy-start.3
  3.8 0.9 copy-start.4
  4.7 0.9 copy-start.5
  5.6 0.7 copy-start.6
  6.3 0.7 copy-start.7
  6.9 0.7 copy-start.8
  7.6 60.7 %copy-start.9 = (bf16[1024,2048]{1,0:T(8,128)(2,1)S(1)}, bf16[1024,2048]{1,0:T(8,128)(2,1)}, u32[]{:S(2)}) copy-start(bf16[1024,2048]{1,0:T(8,128)(2,1)} %param.30) | copy-start | bytes 12582916
  7.6 60.7 %copy-start.10 = (bf16[80,2048]{1,0:T(8,128)(2,1)S(1)}, bf16[80,2048]{1,0:T(8,128)(2,1)}, u32[]{:S(2)}) copy-start(bf16[80,2048]{1,0:T(8,128)(2,1)} %param.19) | copy-start | bytes 983044
  68.3 1.3 copy-start.13
  68.3 2.8 %copy-start.11 = (f32[2048]{0:T(1024)S(1)}, f32[2048]{0:T(1024)}, u32[]{:S(2)}) copy-start(f32[2048]{0:T(1024)} %param.31) | copy-start | bytes 24580
  72.6 78.1 %copy-start.14 = (f32[80,2]{0,1:T(2,128)S(1)}, f32[80,2]{0,1:T(2,128)}, u32[]{:S(2)}) copy-start(f32[80,2]{0,1:T(2,128)} %param.34) | copy-start | bytes 1924
  72.6 80.5 %copy-start.12 = (f32[2048]{0:T(1024)S(1)}, f32[2048]{0:T(1024)}, u32[]{:S(2)}) copy-start(f32[2048]{0:T(1024)} %param.32) | copy-start | bytes 24580

commit v2 on v1

--- a/solution.py
+++ b/solution.py
@@ -72,6 +72,15 @@
     diff = mapped[:, 0] - subtract[:, None, None] * mapped[:, 1]
     normed = diff * lax.rsqrt(jnp.mean(diff * diff, -1, keepdims=True) + 1e-06) * head_gain
     return jnp.transpose(normed, (1, 0, 2)).reshape(diff.shape[1], -1).astype(jnp.bfloat16)
+
+
+def greet(peers):
+    barrier = pltpu.get_barrier_semaphore()
+    for peer in peers:
+        pl.semaphore_signal(
+            barrier, inc=1, device_id=peer, device_id_type=pl.DeviceIdType.MESH
+        )
+    pl.semaphore_wait(barrier, len(peers))
 
 
 def attend_kernel(
@@ -156,8 +165,17 @@
     def kinds_for(target, kinds):
         return [kind for kind in kinds if is_wide(target) or kind not in (1, 4)]
 
+    peers = [{"sp": partner}]
+    for step in range(1, layers):
+        peers.append({"sp": 2 * visit(step) + side})
+    for step in range(layers):
+        for turn in range(1, ranks):
+            peers.append({"sp": 2 * visit(step) + side, "tp": lax.rem(rank + turn, ranks)})
+    greet(peers)
+
+    order = sorted(range(layers), key=lambda index: -is_wide(index))
     for kinds in ((0, 1, 2), (3, 4)):
-        for target in sorted(range(layers), key=lambda index: -is_wide(index)):
+        for target in order if kinds[0] == 0 else reversed(order):
             for kind in kinds_for(target, kinds):
 
                 @pl.when(layer != target)
@@ -311,7 +329,7 @@
             dma((heads,)),
         ],
         compiler_params=pltpu.CompilerParams(
-            has_side_effects=True, vmem_limit_bytes=40 * 1024 * 1024
+            collective_id=0, has_side_effects=True, vmem_limit_bytes=62 * 1024 * 1024
         ),
     )(
         subtract_narrow,
@@ -338,12 +356,25 @@
     )
 
 
+def flip(index, bits, size):
+    flipped, bit = 0, 1
+    while bit < size:
+        one, other = lax.rem(index // bit, 2), lax.rem(bits // bit, 2)
+        flipped = flipped + bit * (one + other - 2 * one * other)
+        bit *= 2
+    return flipped
+
+
 def expert_kernel(
     send_ref,
+    gate_from,
+    up_from,
+    down_from,
+    out_ref,
     gate_ref,
     up_ref,
     down_ref,
-    out_ref,
+    weight_sem,
     rows,
     part,
     pairs,
@@ -382,7 +413,7 @@
         )
 
     def far(hop):
-        target = lax.rem(me + hop, shards)
+        target = flip(me, hop, shards)
         return copy_to(
             at(send_ref, target),
             at(rows, hop * ranks + my_place),
@@ -417,8 +448,21 @@
             at(back, me),
             back_send.at[hop],
             back_recv.at[hop],
-            {"sp": lax.rem(me - hop + shards, shards)},
-        )
+            {"sp": flip(me, hop, shards)},
+        )
+
+    weights = [
+        pltpu.make_async_copy(source, place, weight_sem.at[index])
+        for index, (source, place) in enumerate(
+            zip((gate_from, up_from, down_from), (gate_ref, up_ref, down_ref))
+        )
+    ]
+    for copy in weights:
+        copy.start()
+    greet(
+        [{"tp": partner}, {"tp": across}]
+        + [{"sp": flip(me, hop, shards)} for hop in range(1, shards)]
+    )
 
     @pl.loop(1, shards)
     def _(hop):
@@ -441,6 +485,11 @@
         near(2, hop).start()
 
     def compute(hop):
+        @pl.when(hop == 0)
+        def _():
+            for copy in weights:
+                copy.wait()
+
         near(0, hop).wait_recv()
         near(2, hop).wait_recv()
         span = pl.ds(pl.multiple_of(hop * block, block), block)
@@ -497,13 +546,7 @@
         def _():
             far(hop).wait_send()
             give_back(hop).wait_send()
-            copy_to(
-                at(done, hop),
-                at(back, lax.rem(me + hop, shards)),
-                back_send.at[hop],
-                back_recv.at[hop],
-                {"sp": lax.rem(me + hop, shards)},
-            ).wait_recv()
+            give_back(hop).wait_recv()
 
     out_ref[...] = back[...]
 
@@ -516,9 +559,11 @@
     return pl.pallas_call(
         expert_kernel,
         out_shape=jax.ShapeDtypeStruct((total, width), jnp.bfloat16),
-        in_specs=[vmem] * 4,
+        in_specs=[vmem] + [pl.BlockSpec(memory_space=pl.ANY)] * 3,
         out_specs=vmem,
-        scratch_shapes=[
+        scratch_shapes=[pltpu.VMEM(part.shape, part.dtype) for part in (gate, up, down)]
+        + [dma((3,))]
+        + [
             pltpu.VMEM((count * total, width), jnp.bfloat16)
             for count in (ranks, ranks, 2, 1, 1, 1, 1)
         ]
@@ -533,7 +578,7 @@
             dma((shards,)),
         ],
         compiler_params=pltpu.CompilerParams(
-            has_side_effects=True, vmem_limit_bytes=56 * 1024 * 1024
+            collective_id=1, has_side_effects=True, vmem_limit_bytes=62 * 1024 * 1024
         ),
     )(outgoing, gate, up, down)
 
@@ -615,7 +660,11 @@
     local_rows, top_count = expert_ids.shape
     experts = lax.axis_size("sp")
     capacity = max(2, 3 * local_rows * top_count // (2 * experts))
-    in_kernel = lax.axis_size("tp") == 4 and 4 * experts * capacity * residual.shape[1] < 2**23
+    in_kernel = (
+        lax.axis_size("tp") == 4
+        and experts & (experts - 1) == 0
+        and 4 * experts * capacity * residual.shape[1] < 2**23
+    )
     if in_kernel:
         capacity = -(-capacity // 16) * 16
     flat_ids = expert_ids.reshape(-1)

time: 154 us -> 137 us (0.89); the launches traced: 154 us -> 135 us
  Pallas kernels: 136 us -> 123 us
  local copies, waits for them, and re-layouts: 8.26 us -> 0.97 us
    pallas_call x1, Pallas kernels: 78 us -> 66.1 us  [experts_by_source(): pl.pallas_call(expert_kernel, out_shape=jax.ShapeDtypeStruct((total, widt...]
    unnamed x31 -> x15, local copies, waits for them, and re-layouts: 7.7 us -> 0.41 us
where the time goes in v2:
time: 137 us; the launch traced here: 135 us
  Pallas kernels  123 us (90%)
  matrix products  7.8 us (6%)
  other arithmetic  2.35 us (2%)
    pallas_call x1, Pallas kernels, experts_by_source(): pl.pallas_call(expert_kernel, out_shape=jax.ShapeDtypeStruct((total, widt...  66.1 us
    pallas_call x1, Pallas kernels, attend_by_head(): pl.pallas_call(attend_kernel, out_shape=jax.ShapeDtypeStruct((out_rows, h...  57.3 us
    dot_general x1, matrix products, on_device(): jnp.dot(full_narrow, out_narrow, preferred_element_type=jnp.float32)  3.26 us

profile of v2, /device:TPU:0, one launch (start us, length us, event | category | flops | bytes accessed | tf_op | source)
XLA Modules:
  0.0 134.7 jit_solution(11530201609211663713)
XLA Ops:
  0.0 0.0 copy-start.2
  0.0 57.3 %shard_map.181 = bf16[80,2048]{1,0:T(8,128)(2,1)} custom-call(f32[2]{0:T(128)} %narrow_sub_ref.1, f32[2]{0:T(128)} %wide_sub_ref.1, f32[1,128]{1,0:T(1,128)} %bitcast.18, bf16[320,256]{1,0:T(8,128)(2,1)} %query_narrow_ref.1, bf16[320,256]{1,0:T(8,128)(2,1)} %key_narrow_ref.1, bf16[320,256]{1,0:T(8,128)(2,1)} %value_narrow_ref.1, ...), custom_call_target="tpu_custom_call" | custom-call | tf_op jit(solution)/shard_map/pallas_call | solution.py:313
  57.3 0.0 copy-start
  57.3 0.0 copy-start.1
  57.3 3.3 %fusion.2 = f32[80,2048]{1,0:T(8,128)S(1)} fusion(bf16[1024,2048]{1,0:T(8,128)(2,1)} %param.29, bf16[80,2048]{1,0:T(8,128)(2,1)} %shard_map.181), kind=kOutput, calls=%fused_computation.12 | convolution fusion | flops 335544320 | bytes 5013504 | tf_op jit(solution)/shard_map/dot_general | solution.py:654
  60.6 0.0 copy-done.2
  60.6 0.2 copy-done
  60.9 0.0 copy-done.1
  60.9 0.0 copy-start.5
  60.9 0.0 copy-start.3
  60.9 1.0 fusion.7
  61.9 0.2 multiply_reduce_fusion.1
  62.2 0.0 copy-done.5
  62.2 0.1 copy.32
  62.3 0.1 eq.48
  62.5 0.6 reduce-window.6
  63.0 0.2 slice_reduce_fusion
  63.3 0.1 add_bitcast_fusion
  63.4 0.1 reduce_sum.59
  63.5 0.1 copy.33
  63.6 0.1 fusion.4
  63.7 0.0 copy-done.3
  63.7 1.5 %convolution_convert_fusion.send_ref = bf16[256,2048]{1,0:T(8,128)(2,1)} fusion(pred[256,80]{0,1:T(8,128)(4,1)S(1)} %fusion.4, f32[80,2048]{1,0:T(8,128)S(1)} %get-tuple-element.6, f32[2048]{0:T(1024)S(1)} %copy-done.3, f32[80]{0:T(128)S(1)} %add_rsqrt_fusion.1, f32[80]{0:T(128)S(1)} %broadcast_multiply_fusion.1), kind=kOutput, calls=%fused_computation | convolution fusion | flops 85065728 | bytes 1733248 | tf_op jit(solution)/shard_map/dot_general | solution.py:678
  65.3 0.0 copy-start.6
  65.3 0.0 copy-start.4
  65.3 66.1 %shard_map.182 = bf16[256,2048]{1,0:T(8,128)(2,1)} custom-call(bf16[256,2048]{1,0:T(8,128)(2,1)} %convolution_convert_fusion.send_ref, bf16[2048,512]{1,0:T(8,128)(2,1)} %bitcast.15, bf16[2048,512]{1,0:T(8,128)(2,1)} %bitcast.16, bf16[512,2048]{1,0:T(8,128)(2,1)} %bitcast.17), custom_call_target="tpu_custom_call" | custom-call | tf_op jit(solution)/shard_map/pallas_call | solution.py:559
  131.4 0.0 copy-done.6
  131.4 0.1 select_reduce_fusion
  131.5 2.0 %fusion.8 = (f32[80]{0:T(128)S(1)}, f32[80,2048]{1,0:T(8,128)S(1)}) fusion(f32[80,256]{1,0:T(8,128)S(1)} %select_reduce_fusion, bf16[256,2048]{1,0:T(8,128)(2,1)} %shard_map.182, f32[2048]{0:T(1024)S(1)} %copy-done.3, f32[80]{0:T(128)S(1)} %add_rsqrt_fusion.1, f32[80,2048]{1,0:T(8,128)S(1)} %get-tuple-element.6, f32[80]{0:T(128)S(1)} %broadcast_multiply_fusion.1), kind=kOutput, calls=%fused_computation.29 | convolution fusion | flops 504627136 | bytes 2450368 | tf_op jit(solution)/shard_map/dot_general | solution.py:685
  133.6 0.2 multiply_reduce_fusion
  133.8 0.0 copy-done.4
  133.8 0.9 multiply_convert_fusion
  (10 shorter events, 0.1 us)
Async XLA Ops:
  0.0 60.6 %copy-start.2 = (bf16[80,2048]{1,0:T(8,128)(2,1)S(1)}, bf16[80,2048]{1,0:T(8,128)(2,1)}, u32[]{:S(2)}) copy-start(bf16[80,2048]{1,0:T(8,128)(2,1)} %param.19) | copy-start | bytes 983044
  57.3 3.5 %copy-start = (bf16[1024,2048]{1,0:T(8,128)(2,1)S(1)}, bf16[1024,2048]{1,0:T(8,128)(2,1)}, u32[]{:S(2)}) copy-start(bf16[1024,2048]{1,0:T(8,128)(2,1)} %param.30) | copy-start | bytes 12582916
  57.3 3.6 %copy-start.1 = (bf16[80,2048]{1,0:T(8,128)(2,1)S(1)}, bf16[80,2048]{1,0:T(8,128)(2,1)}, u32[]{:S(2)}) copy-start(bf16[80,2048]{1,0:T(8,128)(2,1)} %shard_map.181) | copy-start | bytes 983044
  60.9 1.3 copy-start.5
  60.9 2.8 %copy-start.3 = (f32[2048]{0:T(1024)S(1)}, f32[2048]{0:T(1024)}, u32[]{:S(2)}) copy-start(f32[2048]{0:T(1024)} %param.31) | copy-start | bytes 24580
  65.3 66.2 %copy-start.6 = (f32[80,2]{0,1:T(2,128)S(1)}, f32[80,2]{0,1:T(2,128)}, u32[]{:S(2)}) copy-start(f32[80,2]{0,1:T(2,128)} %param.34) | copy-start | bytes 1924
  65.3 68.6 %copy-start.4 = (f32[2048]{0:T(1024)S(1)}, f32[2048]{0:T(1024)}, u32[]{:S(2)}) copy-start(f32[2048]{0:T(1024)} %param.32) | copy-start | bytes 24580

commit v3 on v2

--- a/solution.py
+++ b/solution.py
@@ -83,7 +83,8 @@
     pl.semaphore_wait(barrier, len(peers))
 
 
-def attend_kernel(
+def attend_part(
+    meanwhile,
     narrow_sub_ref,
     wide_sub_ref,
     gain_ref,
@@ -93,7 +94,6 @@
     query_wide_ref,
     key_wide_ref,
     value_wide_ref,
-    out_ref,
     query_all,
     key_all,
     value_all,
@@ -167,7 +167,8 @@
 
     peers = [{"sp": partner}]
     for step in range(1, layers):
-        peers.append({"sp": 2 * visit(step) + side})
+        for column in range(2):
+            peers.append({"sp": 2 * visit(step) + column})
     for step in range(layers):
         for turn in range(1, ranks):
             peers.append({"sp": 2 * visit(step) + side, "tp": lax.rem(rank + turn, ranks)})
@@ -189,6 +190,8 @@
                     ).start()
 
     value_all[:, lanes:] = jnp.ones((value_all.shape[0], lanes), jnp.bfloat16)
+
+    meanwhile()
 
     def landed_here(kind, index, half, sem):
         where = place(kind, index, half)
@@ -241,7 +244,7 @@
         return remote, here, (block == me) & (rank == part)
 
     lane = lax.broadcasted_iota(jnp.int32, (tok_rows, lanes), 1)
-    for step in range(layers):
+    for step in list(range(1, layers)) + [0]:
         index = visit(step)
         for kind in (3, 4):
             when_mine(kind, lambda: landed_here(kind, index, side, recv_sem))
@@ -278,70 +281,29 @@
             def _():
                 remote.start()
 
-    for target in range(layers):
-        for kind in kinds_for(target, range(5)):
-
-            @pl.when(layer != target)
-            def _():
-                to_layer(kind, target).wait_send()
-
-    for index in range(layers):
-        for kind in range(3):
-            when_mine(kind, lambda: pass_on(kind, index).wait_send())
-        for part in range(ranks):
-            remote, here, mine = to_tokens(index, part)
-
-            @pl.when(jnp.logical_not(mine))
-            def _():
-                remote.wait_send()
-
     for head in range(layers * ranks):
         where = landed.at[:, pl.ds(head * lanes, lanes)]
         pltpu.make_async_copy(where, where, out_recv.at[head]).wait()
-    out_ref[...] = landed[...]
-
-
-def attend_by_head(queries, keys, values, subtract_narrow, subtract_wide, head_gain, out_rows):
-    shards, ranks = lax.axis_size("sp"), lax.axis_size("tp")
-    head_count, lanes = subtract_narrow.shape[0], head_gain.shape[0]
-    tok_rows = keys[0].shape[0]
-    tokens, layers = shards * tok_rows, 2 * head_count
-    heads = layers * ranks
-    vmem = pl.BlockSpec(memory_space=pltpu.VMEM)
-    smem = pl.BlockSpec(memory_space=pltpu.SMEM)
-    dma = pltpu.SemaphoreType.DMA
-    return pl.pallas_call(
-        attend_kernel,
-        out_shape=jax.ShapeDtypeStruct((out_rows, heads * lanes), jnp.bfloat16),
-        in_specs=[smem, smem, vmem] + [pl.BlockSpec(memory_space=pl.ANY)] * 6,
-        out_specs=vmem,
-        scratch_shapes=[
-            pltpu.VMEM((2, layers * tok_rows, lanes), jnp.bfloat16),
-            pltpu.VMEM((2, tokens, lanes), jnp.bfloat16),
-            pltpu.VMEM((tokens, 2 * lanes), jnp.bfloat16),
-            pltpu.VMEM((layers * tok_rows, lanes), jnp.bfloat16),
-            pltpu.VMEM((out_rows, heads * lanes), jnp.bfloat16),
-            dma((5, layers)),
-            dma((5, layers)),
-            dma((3, layers)),
-            dma((3, layers)),
-            dma((layers, ranks)),
-            dma((heads,)),
-        ],
-        compiler_params=pltpu.CompilerParams(
-            collective_id=0, has_side_effects=True, vmem_limit_bytes=62 * 1024 * 1024
-        ),
-    )(
-        subtract_narrow,
-        subtract_wide,
-        head_gain[None],
-        queries[0],
-        keys[0],
-        values[0],
-        queries[1],
-        keys[1],
-        values[1],
-    )
+
+    def drain():
+        for target in range(layers):
+            for kind in kinds_for(target, range(5)):
+
+                @pl.when(layer != target)
+                def _():
+                    to_layer(kind, target).wait_send()
+
+        for index in range(layers):
+            for kind in range(3):
+                when_mine(kind, lambda: pass_on(kind, index).wait_send())
+            for part in range(ranks):
+                remote, here, mine = to_tokens(index, part)
+
+                @pl.when(jnp.logical_not(mine))
+                def _():
+                    remote.wait_send()
+
+    return drain
 
 
 def head_split_fits(tok_rows, out_rows, ranks, heads, shards, value_size, key_sizes):
@@ -365,16 +327,12 @@
     return flipped
 
 
-def expert_kernel(
+def expert_part(
+    weights,
     send_ref,
-    gate_from,
-    up_from,
-    down_from,
-    out_ref,
     gate_ref,
     up_ref,
     down_ref,
-    weight_sem,
     rows,
     part,
     pairs,
@@ -451,19 +409,6 @@
             {"sp": flip(me, hop, shards)},
         )
 
-    weights = [
-        pltpu.make_async_copy(source, place, weight_sem.at[index])
-        for index, (source, place) in enumerate(
-            zip((gate_from, up_from, down_from), (gate_ref, up_ref, down_ref))
-        )
-    ]
-    for copy in weights:
-        copy.start()
-    greet(
-        [{"tp": partner}, {"tp": across}]
-        + [{"sp": flip(me, hop, shards)} for hop in range(1, shards)]
-    )
-
     @pl.loop(1, shards)
     def _(hop):
         far(hop).start()
@@ -548,25 +493,190 @@
             give_back(hop).wait_send()
             give_back(hop).wait_recv()
 
-    out_ref[...] = back[...]
-
-
-def experts_by_source(outgoing, gate, up, down):
+
+def norm_rows(values):
+    center = jnp.mean(values, -1, keepdims=True)
+    spread = jnp.mean(jnp.square(values - center), -1, keepdims=True)
+    return (values - center) * lax.rsqrt(spread + 1e-05)
+
+
+def layer_kernel(
+    narrow_sub_ref,
+    wide_sub_ref,
+    gain_ref,
+    residual_ref,
+    norm1_ref,
+    ids_ref,
+    choice_ref,
+    query_narrow_ref,
+    key_narrow_ref,
+    value_narrow_ref,
+    query_wide_ref,
+    key_wide_ref,
+    value_wide_ref,
+    narrow_from,
+    wide_from,
+    gate_from,
+    up_from,
+    down_from,
+    out_ref,
+    mix_weight,
+    gate_ref,
+    up_ref,
+    down_ref,
+    hidden,
+    send_ref,
+    table,
+    combine,
+    ids_wide,
+    choice_wide,
+    mix_sem,
+    weight_sem,
+    *scratch,
+):
+    attend_scratch, expert_scratch = scratch[:11], scratch[11:]
+    landed = attend_scratch[4]
+    back = expert_scratch[6]
+    top_count, rows = ids_ref.shape
+    columns = table.shape[1]
+    experts = lax.axis_size("sp")
+    total = send_ref.shape[0]
+    capacity = total // experts
+    depth = narrow_from.shape[0]
+
+    def fetch(source, place, sem):
+        copy = pltpu.make_async_copy(source, place, sem)
+        copy.start()
+        return copy
+
+    mixers = [
+        fetch(narrow_from, mix_weight.at[pl.ds(0, depth), :], mix_sem.at[0]),
+        fetch(wide_from, mix_weight.at[pl.ds(depth, depth), :], mix_sem.at[1]),
+    ]
+    weights = [
+        fetch(gate_from, gate_ref, weight_sem.at[0]),
+        fetch(up_from, up_ref, weight_sem.at[1]),
+        fetch(down_from, down_ref, weight_sem.at[2]),
+    ]
+
+    def route():
+        ids_wide[...] = jnp.full(ids_wide.shape, -1, jnp.int32)
+        ids_wide[:, pl.ds(0, rows)] = ids_ref[...]
+        choice_wide[...] = jnp.zeros_like(choice_wide)
+        choice_wide[:, pl.ds(0, rows)] = choice_ref[...]
+        ids = [ids_wide[pl.ds(choice, 1), :] for choice in range(top_count)]
+        expert = lax.broadcasted_iota(jnp.int32, (experts, columns), 0)
+        named = [(index == expert).astype(jnp.float32) for index in ids]
+        later = lax.broadcasted_iota(jnp.int32, (columns, columns), 0) < lax.broadcasted_iota(
+            jnp.int32, (columns, columns), 1
+        )
+        before = jnp.dot(
+            sum(named).astype(jnp.bfloat16),
+            later.astype(jnp.float32).astype(jnp.bfloat16),
+            preferred_element_type=jnp.float32,
+        )
+        line = lax.broadcasted_iota(jnp.int32, (total, columns), 0)
+        picks = jnp.zeros((total, columns), jnp.float32)
+        mixing = jnp.zeros((total, columns), jnp.float32)
+        for choice in range(top_count):
+            held = jnp.sum(before * named[choice], 0, keepdims=True).astype(jnp.int32)
+            taken = (ids[choice] * capacity + held == line) & (ids[choice] >= 0)
+            picks = jnp.where(taken, 1.0, picks)
+            mixing = jnp.where(taken, choice_wide[pl.ds(choice, 1), :], mixing)
+        table[...] = picks.astype(jnp.bfloat16)
+        combine[...] = mixing.T
+        hidden[...] = jnp.zeros_like(hidden)
+
+    drain = attend_part(
+        route,
+        narrow_sub_ref,
+        wide_sub_ref,
+        gain_ref,
+        query_narrow_ref,
+        key_narrow_ref,
+        value_narrow_ref,
+        query_wide_ref,
+        key_wide_ref,
+        value_wide_ref,
+        *attend_scratch,
+    )
+    for copy in mixers:
+        copy.wait()
+    mix = jnp.dot(landed[...], mix_weight[...], preferred_element_type=jnp.float32)
+    held = residual_scale * residual_ref[...].astype(jnp.float32) + mix
+    hidden[pl.ds(0, rows), :] = (norm_rows(held) * norm1_ref[...]).astype(jnp.bfloat16)
+    send_ref[...] = jnp.dot(
+        table[...], hidden[...], preferred_element_type=jnp.float32
+    ).astype(jnp.bfloat16)
+    expert_part(weights, send_ref, gate_ref, up_ref, down_ref, *expert_scratch)
+    coarse = combine[...].astype(jnp.bfloat16)
+    fine = (combine[...] - coarse.astype(jnp.float32)).astype(jnp.bfloat16)
+    routed = jnp.dot(coarse, back[...], preferred_element_type=jnp.float32) + jnp.dot(
+        fine, back[...], preferred_element_type=jnp.float32
+    )
+    tokens = residual_scale * hidden[pl.ds(0, rows), :].astype(jnp.float32) + routed[:rows]
+    out_ref[...] = norm_rows(tokens)
+    drain()
+
+
+def whole_layer(
+    residual,
+    attend_args,
+    subtract_narrow,
+    subtract_wide,
+    head_gain,
+    out_weights,
+    norm1_gain,
+    norm2_gain,
+    expert_ids,
+    expert_weight,
+    expert_weights,
+    capacity,
+):
     shards, ranks = lax.axis_size("sp"), lax.axis_size("tp")
-    total, width = outgoing.shape
+    head_count, lanes = subtract_narrow.shape[0], head_gain.shape[0]
+    tok_rows = attend_args[0].shape[0]
+    rows, width = residual.shape
+    tokens, layers = shards * tok_rows, 2 * head_count
+    heads = layers * ranks
+    total = shards * capacity
     vmem = pl.BlockSpec(memory_space=pltpu.VMEM)
+    smem = pl.BlockSpec(memory_space=pltpu.SMEM)
     dma = pltpu.SemaphoreType.DMA
-    return pl.pallas_call(
-        expert_kernel,
-        out_shape=jax.ShapeDtypeStruct((total, width), jnp.bfloat16),
-        in_specs=[vmem] + [pl.BlockSpec(memory_space=pl.ANY)] * 3,
+
+    def buffer(*shape):
+        return pltpu.VMEM(shape, jnp.bfloat16)
+
+    columns = -(-rows // 128) * 128
+    normed = pl.pallas_call(
+        layer_kernel,
+        out_shape=jax.ShapeDtypeStruct((rows, width), jnp.float32),
+        in_specs=[smem, smem] + [vmem] * 5 + [pl.BlockSpec(memory_space=pl.ANY)] * 11,
         out_specs=vmem,
-        scratch_shapes=[pltpu.VMEM(part.shape, part.dtype) for part in (gate, up, down)]
-        + [dma((3,))]
+        scratch_shapes=[buffer(heads * lanes, width)]
+        + [buffer(*part.shape) for part in expert_weights]
         + [
-            pltpu.VMEM((count * total, width), jnp.bfloat16)
-            for count in (ranks, ranks, 2, 1, 1, 1, 1)
+            buffer(columns, width),
+            buffer(total, width),
+            buffer(total, columns),
+            pltpu.VMEM((columns, total), jnp.float32),
+            pltpu.VMEM(expert_ids.shape[1:] + (columns,), jnp.int32),
+            pltpu.VMEM(expert_ids.shape[1:] + (columns,), jnp.float32),
+            dma((2,)),
+            dma((3,)),
+            buffer(2, layers * tok_rows, lanes),
+            buffer(2, tokens, lanes),
+            buffer(tokens, 2 * lanes),
+            buffer(layers * tok_rows, lanes),
+            buffer(rows, heads * lanes),
+            dma((5, layers)),
+            dma((5, layers)),
+            dma((3, layers)),
+            dma((3, layers)),
+            dma((layers, ranks)),
+            dma((heads,)),
         ]
+        + [buffer(count * total, width) for count in (ranks, ranks, 2, 1, 1, 1, 1)]
         + [
             dma((shards,)),
             dma((shards,)),
@@ -578,9 +688,21 @@
             dma((shards,)),
         ],
         compiler_params=pltpu.CompilerParams(
-            collective_id=1, has_side_effects=True, vmem_limit_bytes=62 * 1024 * 1024
+            collective_id=0, has_side_effects=True, vmem_limit_bytes=62 * 1024 * 1024
         ),
-    )(outgoing, gate, up, down)
+    )(
+        subtract_narrow,
+        subtract_wide,
+        head_gain[None],
+        residual,
+        norm1_gain[None],
+        expert_ids.T,
+        expert_weight.T,
+        *attend_args,
+        *out_weights,
+        *expert_weights,
+    )
+    return (normed * norm2_gain).astype(jnp.bfloat16)
 
 
 def on_device(
@@ -607,66 +729,69 @@
     tok_rows = query_narrow.shape[0]
     head_count = subtract_narrow.shape[0]
     value_size = head_gain.shape[0]
-    if head_split_fits(
-        tok_rows,
-        residual.shape[0],
-        lax.axis_size("tp"),
-        head_count,
-        lax.axis_size("sp"),
-        value_size,
-        tuple(part.shape[1] // (2 * head_count) for part in (key_narrow, key_wide)),
+    local_rows, top_count = expert_ids.shape
+    experts = lax.axis_size("sp")
+    capacity = max(2, 3 * local_rows * top_count // (2 * experts))
+    padded = -(-capacity // 16) * 16
+    if (
+        head_split_fits(
+            tok_rows,
+            local_rows,
+            lax.axis_size("tp"),
+            head_count,
+            experts,
+            value_size,
+            tuple(part.shape[1] // (2 * head_count) for part in (key_narrow, key_wide)),
+        )
+        and lax.axis_size("tp") == 4
+        and top_count == 2
+        and experts & (experts - 1) == 0
+        and 4 * experts * padded * residual.shape[1] < 2**23
     ):
-        attended = attend_by_head(
-            (query_narrow, query_wide),
-            (key_narrow, key_wide),
-            (value_narrow, value_wide),
+        return whole_layer(
+            residual,
+            (query_narrow, key_narrow, value_narrow, query_wide, key_wide, value_wide),
             subtract_narrow,
             subtract_wide,
             head_gain,
-            residual.shape[0],
-        )
-        full_narrow, full_wide = jnp.split(attended, 2, 1)
-    else:
-        narrow_queries = query_narrow.reshape(tok_rows, head_count, 2, -1)
-        wide_queries = query_wide.reshape(tok_rows, head_count, 2, -1)
-        narrow_start = start_carry(head_count, tok_rows, value_size)
-        wide_start = start_carry(head_count, tok_rows, value_size)
-        narrow_state = absorb_keys(
-            narrow_start,
-            narrow_queries,
-            lax.all_gather(key_narrow, "sp", axis=0, tiled=True),
-            lax.all_gather(value_narrow, "sp", axis=0, tiled=True),
-            tok_rows,
-        )
-        wide_state = absorb_keys(
-            wide_start,
-            wide_queries,
-            lax.all_gather(key_wide, "sp", axis=0, tiled=True),
-            lax.all_gather(value_wide, "sp", axis=0, tiled=True),
-            tok_rows,
-        )
-        attended_narrow = finish_heads(narrow_state, subtract_narrow, head_gain)
-        attended_wide = finish_heads(wide_state, subtract_wide, head_gain)
-        full_narrow, full_wide = (
-            lax.all_to_all(attended_narrow, "tp", split_axis=0, concat_axis=1, tiled=True),
-            lax.all_to_all(attended_wide, "tp", split_axis=0, concat_axis=1, tiled=True),
-        )
+            (out_narrow, out_wide),
+            norm1_gain,
+            norm2_gain,
+            expert_ids,
+            expert_weight,
+            (gate_proj[0], up_proj[0], down_proj[0]),
+            padded,
+        )
+    narrow_queries = query_narrow.reshape(tok_rows, head_count, 2, -1)
+    wide_queries = query_wide.reshape(tok_rows, head_count, 2, -1)
+    narrow_start = start_carry(head_count, tok_rows, value_size)
+    wide_start = start_carry(head_count, tok_rows, value_size)
+    narrow_state = absorb_keys(
+        narrow_start,
+        narrow_queries,
+        lax.all_gather(key_narrow, "sp", axis=0, tiled=True),
+        lax.all_gather(value_narrow, "sp", axis=0, tiled=True),
+        tok_rows,
+    )
+    wide_state = absorb_keys(
+        wide_start,
+        wide_queries,
+        lax.all_gather(key_wide, "sp", axis=0, tiled=True),
+        lax.all_gather(value_wide, "sp", axis=0, tiled=True),
+        tok_rows,
+    )
+    attended_narrow = finish_heads(narrow_state, subtract_narrow, head_gain)
+    attended_wide = finish_heads(wide_state, subtract_wide, head_gain)
+    full_narrow, full_wide = (
+        lax.all_to_all(attended_narrow, "tp", split_axis=0, concat_axis=1, tiled=True),
+        lax.all_to_all(attended_wide, "tp", split_axis=0, concat_axis=1, tiled=True),
+    )
     mix = jnp.dot(full_narrow, out_narrow, preferred_element_type=jnp.float32) + jnp.dot(
         full_wide, out_wide, preferred_element_type=jnp.float32
     )
     hidden = layer_norm(residual_scale * residual.astype(jnp.float32) + mix, norm1_gain).astype(
         jnp.bfloat16
     )
-    local_rows, top_count = expert_ids.shape
-    experts = lax.axis_size("sp")
-    capacity = max(2, 3 * local_rows * top_count // (2 * experts))
-    in_kernel = (
-        lax.axis_size("tp") == 4
-        and experts & (experts - 1) == 0
-        and 4 * experts * capacity * residual.shape[1] < 2**23
-    )
-    if in_kernel:
-        capacity = -(-capacity // 16) * 16
     flat_ids = expert_ids.reshape(-1)
     onehot = (flat_ids[:, None] == jnp.arange(experts, dtype=jnp.int32)[None, :]).astype(jnp.int32)
     before = jnp.cumsum(onehot, 0) - onehot
@@ -678,35 +803,27 @@
     outgoing = jnp.dot(dispatch_table, hidden, preferred_element_type=jnp.float32).astype(
         jnp.bfloat16
     )
-    if in_kernel:
-        returned_flat = experts_by_source(outgoing, gate_proj[0], up_proj[0], down_proj[0])
-        named = slots[..., None] == jnp.arange(experts * capacity, dtype=jnp.int32)
-        combine = jnp.sum(jnp.where(named, expert_weight[..., None], 0.0), 1)
-        routed = jnp.dot(
-            combine, returned_flat.astype(jnp.float32), precision=lax.Precision.HIGHEST
-        )
-    else:
-        outgoing = outgoing.reshape(experts, capacity, -1)
-        gathered = lax.all_gather(
-            lax.all_to_all(outgoing, "sp", split_axis=0, concat_axis=0, tiled=True),
-            "tp",
-            axis=1,
-            tiled=True,
-        )
-        flat_rows = gathered.reshape(-1, gathered.shape[2])
-        gate_part = jnp.dot(flat_rows, gate_proj[0], preferred_element_type=jnp.float32)
-        up_part = jnp.dot(flat_rows, up_proj[0], preferred_element_type=jnp.float32)
-        inner = (jax.nn.silu(gate_part) * up_part).astype(jnp.bfloat16)
-        partial_out = jnp.dot(inner, down_proj[0], preferred_element_type=jnp.float32).reshape(
-            gathered.shape
-        )
-        summed = lax.psum_scatter(
-            partial_out.astype(jnp.bfloat16), "tp", scatter_dimension=1, tiled=True
-        )
-        returned = lax.all_to_all(summed, "sp", split_axis=0, concat_axis=0, tiled=True)
-        returned_flat = returned.reshape(experts * capacity, -1)
-        picked = returned_flat[slots].astype(jnp.float32)
-        routed = jnp.sum(expert_weight[..., None] * picked, 1)
+    outgoing = outgoing.reshape(experts, capacity, -1)
+    gathered = lax.all_gather(
+        lax.all_to_all(outgoing, "sp", split_axis=0, concat_axis=0, tiled=True),
+        "tp",
+        axis=1,
+        tiled=True,
+    )
+    flat_rows = gathered.reshape(-1, gathered.shape[2])
+    gate_part = jnp.dot(flat_rows, gate_proj[0], preferred_element_type=jnp.float32)
+    up_part = jnp.dot(flat_rows, up_proj[0], preferred_element_type=jnp.float32)
+    inner = (jax.nn.silu(gate_part) * up_part).astype(jnp.bfloat16)
+    partial_out = jnp.dot(inner, down_proj[0], preferred_element_type=jnp.float32).reshape(
+        gathered.shape
+    )
+    summed = lax.psum_scatter(
+        partial_out.astype(jnp.bfloat16), "tp", scatter_dimension=1, tiled=True
+    )
+    returned = lax.all_to_all(summed, "sp", split_axis=0, concat_axis=0, tiled=True)
+    returned_flat = returned.reshape(experts * capacity, -1)
+    picked = returned_flat[slots].astype(jnp.float32)
+    routed = jnp.sum(expert_weight[..., None] * picked, 1)
     return layer_norm(residual_scale * hidden.astype(jnp.float32) + routed, norm2_gain).astype(
         jnp.bfloat16
     )

time: 137 us -> 126 us (0.920)
  matrix products: 7.8 us -> 0 us
    dot_general x4 -> x0, matrix products: 7.8 us -> none  [the longest x1 3.26 us: on_device(): jnp.dot(full_narrow, out_narrow, preferred_element_type=jnp.float32)]
    pallas_call x2 -> x1, Pallas kernels: 123 us -> 122 us  [whole_layer(): pl.pallas_call(layer_kernel, out_shape=jax.ShapeDtypeStruct((rows, width)...]
where the time goes in v3:
time: 126 us; the launch traced here: 124 us
  Pallas kernels  122 us (97%)
  other arithmetic  1.86 us (1%)
    pallas_call x1, Pallas kernels, whole_layer(): pl.pallas_call(layer_kernel, out_shape=jax.ShapeDtypeStruct((rows, width)...  122 us

profile of v3, /device:TPU:0, one launch (start us, length us, event | category | flops | bytes accessed | tf_op | source)
XLA Modules:
  0.0 123.5 jit_solution(17852061443468152494)
XLA Ops:
  0.0 0.0 copy-start
  0.0 121.6 %shard_map.181 = f32[80,2048]{1,0:T(8,128)} custom-call(f32[2]{0:T(128)} %narrow_sub_ref.1, f32[2]{0:T(128)} %wide_sub_ref.1, f32[1,128]{1,0:T(1,128)} %bitcast.13, bf16[80,2048]{1,0:T(8,128)(2,1)} %residual_ref.1, f32[1,2048]{1,0:T(1,128)} %bitcast.10, s32[2,80]{1,0:T(2,128)} %bitcast.11, f32[2,80]{1,0:T(2,128)} %bitcast.12, ...), custom_call_target="tpu_custom_call" | custom-call | tf_op jit(solution)/shard_map/pallas_call | solution.py:651
  121.7 0.0 copy-done
  121.7 1.9 %multiply_convert_fusion = bf16[80,2048]{1,0:T(8,128)(2,1)} fusion(f32[80,2048]{1,0:T(8,128)} %shard_map.181, f32[2048]{0:T(1024)S(1)} %copy-done), kind=kLoop, calls=%fused_computation | loop fusion | flops 327680 | bytes 991232 | tf_op jit(solution)/shard_map/convert_element_type | solution.py:705
Async XLA Ops:
  0.0 121.7 %copy-start = (f32[2048]{0:T(1024)S(1)}, f32[2048]{0:T(1024)}, u32[]{:S(2)}) copy-start(f32[2048]{0:T(1024)} %param.32) | copy-start | bytes 24580

commit v4 on v3

--- a/solution.py
+++ b/solution.py
@@ -318,6 +318,10 @@
     )
 
 
+def hop_bits(hop):
+    return 4 * lax.rem(hop, 2) + 2 * lax.rem(hop // 2, 2) + hop // 4
+
+
 def flip(index, bits, size):
     flipped, bit = 0, 1
     while bit < size:
@@ -371,7 +375,7 @@
         )
 
     def far(hop):
-        target = flip(me, hop, shards)
+        target = flip(me, hop_bits(hop), shards)
         return copy_to(
             at(send_ref, target),
             at(rows, hop * ranks + my_place),
@@ -406,7 +410,7 @@
             at(back, me),
             back_send.at[hop],
             back_recv.at[hop],
-            {"sp": flip(me, hop, shards)},
+            {"sp": flip(me, hop_bits(hop), shards)},
         )
 
     @pl.loop(1, shards)
@@ -465,11 +469,11 @@
         def _():
             give_back(hop).start()
 
-    stages = (share, relay, compute, add_pair, finish)
-
-    @pl.loop(0, shards + len(stages) - 1)
+    stages = ((share, 0), (relay, 2), (compute, 3), (add_pair, 4), (finish, 6))
+
+    @pl.loop(0, shards + stages[-1][1])
     def _(step):
-        for late, stage in enumerate(stages):
+        for stage, late in stages:
             hop = step - late
 
             @pl.when((hop >= 0) & (hop < shards))

time: 126 us -> 118 us (0.937); the launches traced: 124 us -> 118 us
  Pallas kernels: 122 us -> 116 us
    pallas_call x1, Pallas kernels: 122 us -> 116 us  [whole_layer(): pl.pallas_call(layer_kernel, out_shape=jax.ShapeDtypeStruct((rows, width)...]
where the time goes in v4:
time: 118 us
  Pallas kernels  116 us (98%)
  other arithmetic  1.86 us (2%)
    pallas_call x1, Pallas kernels, whole_layer(): pl.pallas_call(layer_kernel, out_shape=jax.ShapeDtypeStruct((rows, width)...  116 us

profile of v4, /device:TPU:0, one launch (start us, length us, event | category | flops | bytes accessed | tf_op | source)
XLA Modules:
  0.0 117.7 jit_solution(8954689953424928981)
XLA Ops:
  0.0 0.0 copy-start
  0.0 115.8 %shard_map.181 = f32[80,2048]{1,0:T(8,128)} custom-call(f32[2]{0:T(128)} %narrow_sub_ref.1, f32[2]{0:T(128)} %wide_sub_ref.1, f32[1,128]{1,0:T(1,128)} %bitcast.13, bf16[80,2048]{1,0:T(8,128)(2,1)} %residual_ref.1, f32[1,2048]{1,0:T(1,128)} %bitcast.10, s32[2,80]{1,0:T(2,128)} %bitcast.11, f32[2,80]{1,0:T(2,128)} %bitcast.12, ...), custom_call_target="tpu_custom_call" | custom-call | tf_op jit(solution)/shard_map/pallas_call | solution.py:655
  115.8 0.0 copy-done
  115.8 1.9 %multiply_convert_fusion = bf16[80,2048]{1,0:T(8,128)(2,1)} fusion(f32[80,2048]{1,0:T(8,128)} %shard_map.181, f32[2048]{0:T(1024)S(1)} %copy-done), kind=kLoop, calls=%fused_computation | loop fusion | flops 327680 | bytes 991232 | tf_op jit(solution)/shard_map/convert_element_type | solution.py:709
Async XLA Ops:
  0.0 115.8 %copy-start = (f32[2048]{0:T(1024)S(1)}, f32[2048]{0:T(1024)}, u32[]{:S(2)}) copy-start(f32[2048]{0:T(1024)} %param.32) | copy-start | bytes 24580
